TPU v7x, 256 devices: a whole 4x4x8 slice. The times are simulated.
256 devices in a mesh: sp: 64 (over z, y, core), tp: 4 (over x).
Axes of the slice: x: 4, y: 4, z: 8, core: 2. Of those that a mesh axis runs over, the one named last changes fastest.
Arguments:
- resid: bfloat16 [16384, 2048], P(('sp', 'tp')), may hold values from -6 to 6
- mix_in: bfloat16 [16384, 512], P('sp', 'tp'), may hold values from -6 to 6
- decay_rate: float32 [32, 64], P('tp'), may hold values from -0.05 to 0, as said below
- turn_rate: float32 [32, 64], P('tp'), may hold values from -3.140625 to 3.140625
- forget: float32 [16384, 32], P('sp', 'tp'), may hold values from -2 to 0, as said below
- input_real: float32 [32, 64, 16], P('tp'), may hold values from -1 to 1
- input_imag: float32 [32, 64, 16], P('tp'), may hold values from -1 to 1
- output_real: float32 [32, 16, 64], P('tp'), may hold values from -0.75 to 0.75
- output_imag: float32 [32, 16, 64], P('tp'), may hold values from -0.75 to 0.75
- skip_gain: float32 [32, 16], P('tp'), may hold values from -5 to 5
- mix_gain: float32 [512], replicated, may hold values from 0.1 to 1.9
- w_out: bfloat16 [512, 2048], replicated, may hold values from -0.25 to 0.25
- ffn_gain: float32 [2048], replicated, may hold values from 0.1 to 1.9
- gating_matrix: bfloat16 [2048, 5632], P('sp', 'tp'), may hold values from -0.125 to 0.125
- w_up: bfloat16 [2048, 5632], P('sp', 'tp'), may hold values from -0.125 to 0.125
- w_down: bfloat16 [5632, 2048], P('tp', 'sp'), may hold values from -0.078125 to 0.078125
Outputs:
- result: bfloat16 [16384, 2048], P(('sp', 'tp'))
Inputs may be any that keep to these rules, and one draw needn't show every extreme that they name: `decay_rate`: every entry is negative. `forget`: every entry is at most zero.
All inputs are finite; a program needn't handle non-finite values.
Results may differ from a plain program's by a relative error of at most 0.012.
Values may be sent and summed in bfloat16 or wider, within the bound.
A program may use at most 128 MiB of HBM per device.

v0:
```python
import jax
import jax.numpy as jnp
from jax import lax
from jax.sharding import PartitionSpec as P

eps = 1e-06


def rows_first(arrays, axis, dims):
    turned = [jnp.moveaxis(a, dim, 0) for a, dim in zip(arrays, dims)]
    widths = [t[0].size for t in turned]
    both = jnp.concatenate([t.reshape(-1, w) for t, w in zip(turned, widths)], axis=1)
    filled = lax.all_gather(both, axis, axis=0, tiled=True)
    tiles = jnp.split(filled, [sum(widths[:k]) for k in range(1, len(widths))], axis=1)
    return tuple(
        (
            jnp.moveaxis(b.reshape(-1, *t.shape[1:]), 0, dim)
            for b, t, dim in zip(tiles, turned, dims)
        )
    )


def sent_to_all(value, axis):
    length = lax.axis_size(axis)
    return lax.all_to_all(
        jnp.broadcast_to(value[None], (length, *value.shape)), axis, 0, 0, tiled=True
    )


def gathered_once(value, axis):
    leaves = jax.tree.leaves(value)
    order = sorted(range(len(leaves)), key=lambda k: -leaves[k].size)
    width = (1, *leaves[order[0]].shape)[-1]
    lines = [
        jnp.pad(leaves[k].reshape(-1), (0, -leaves[k].size % width)).reshape(-1, width)
        for k in order
    ]
    both, at, found = (sent_to_all(jnp.concatenate(lines), axis), 0, {})
    for k, line in zip(order, lines):
        piece = both[:, at : at + len(line)].reshape(len(both), -1)
        found[k] = piece[:, : leaves[k].size].reshape(-1, *leaves[k].shape)
        at += len(line)
    numbers = iter(range(len(leaves)))
    return jax.tree.map(lambda _: found[next(numbers)], value)


def joined_by_halves(pieces, combine):
    while len(jax.tree.leaves(pieces)[0]) > 1:
        pieces = jax.vmap(combine)(
            *(jax.tree.map(lambda part: part[side::2], pieces) for side in (0, 1))
        )
    return jax.tree.map(lambda part: part[0], pieces)


def entering(value, axis, combine, identity):
    length, position = (lax.axis_size(axis), lax.axis_index(axis))
    passed = jnp.arange(length) < position

    def kept(part, zero, own):
        part = jnp.where(
            passed.reshape(-1, *(1 for _ in own.shape)), part, jnp.asarray(zero, own.dtype)
        )
        return part

    pieces = gathered_once(value, axis)
    return joined_by_halves(jax.tree.map(kept, pieces, identity, value), combine)


def in_order(tiles, dim):
    tiles = jnp.moveaxis(tiles, 0, dim)
    lengths = tiles.shape
    return tiles.reshape(*lengths[:dim], lengths[dim] * lengths[dim + 1], *lengths[dim + 2 :])


def collect(value, axis, dim):
    tiles = sent_to_all(value, axis)
    return in_order(tiles, dim)


def cut_along(value, dim, length):
    lengths = value.shape
    tiles = value.reshape(*lengths[:dim], length, lengths[dim] // length, *lengths[dim + 1 :])
    return jnp.moveaxis(tiles, dim, 0)


def sent_and_summed(value, axis, dim):
    tiles = cut_along(value, dim, lax.axis_size(axis))
    arrived = lax.all_to_all(tiles, axis, split_axis=0, concat_axis=0, tiled=True)
    return arrived.astype(jnp.float32).sum(axis=0)


def chain(earlier, later):
    first_real, first_imag, push_real, push_imag = earlier
    next_real, next_imag, add_real, add_imag = later
    return (
        next_real * first_real - next_imag * first_imag,
        next_real * first_imag + next_imag * first_real,
        next_real * push_real - next_imag * push_imag + add_real,
        next_real * push_imag + next_imag * push_real + add_imag,
    )


def local_states(log_step, push_real, push_imag, turn):
    high = lax.Precision.DEFAULT
    n_rows, columns = log_step.shape
    span = min(32, n_rows)
    n_spans = n_rows // span
    place = jnp.arange(span, dtype=jnp.float32)
    lower = place[:, None] >= place[None, :]
    lower_cube = lower[:, :, None]
    triangle = lower.astype(jnp.float32)
    lag_angle = (place[:, None] - place[None, :])[:, :, None] * turn[None, None, :]
    lag_cos = jnp.where(lower_cube, jnp.cos(lag_angle), 0.0)
    lag_sin = jnp.where(lower_cube, jnp.sin(lag_angle), 0.0)
    ahead = place + 1.0
    own_cos = jnp.cos(ahead[:, None] * turn[None, :])
    own_sin = jnp.sin(ahead[:, None] * turn[None, :])

    def advance(carry, blocks):
        run_log, state_real, state_imag, offset = carry
        log_block, real_block, imag_block = blocks
        inner = jnp.dot(triangle, log_block, precision=high)
        spread = jnp.where(lower_cube, inner[:, None, :] - inner[None, :, :], 0.0)
        weight = jnp.where(lower_cube, jnp.exp(spread), 0.0)
        weight_real = weight * lag_cos
        weight_imag = weight * lag_sin
        new_real = jnp.sum(weight_real * real_block[None] - weight_imag * imag_block[None], axis=1)
        new_imag = jnp.sum(weight_real * imag_block[None] + weight_imag * real_block[None], axis=1)
        fade = jnp.exp(inner)
        carry_real = fade * own_cos
        carry_imag = fade * own_sin
        new_real = new_real + carry_real * state_real[None] - carry_imag * state_imag[None]
        new_imag = new_imag + carry_real * state_imag[None] + carry_imag * state_real[None]
        whole_fade = jnp.exp(run_log[None] + inner)
        whole_angle = (offset + ahead)[:, None] * turn[None, :]
        prefix_real = whole_fade * jnp.cos(whole_angle)
        prefix_imag = whole_fade * jnp.sin(whole_angle)
        following = (run_log + inner[-1], new_real[-1], new_imag[-1], offset + span)
        return (following, (new_real, new_imag, prefix_real, prefix_imag))

    zero_row = jnp.zeros((columns,), jnp.float32)
    start = (zero_row, zero_row, zero_row, jnp.zeros((), jnp.float32))
    blocks = (
        log_step.reshape(n_spans, span, columns),
        push_real.reshape(n_spans, span, columns),
        push_imag.reshape(n_spans, span, columns),
    )
    final, outputs = lax.scan(advance, start, blocks)
    outputs = tuple((item.reshape(n_rows, columns) for item in outputs))
    total_fade = jnp.exp(final[0])
    totals = (
        total_fade * jnp.cos(n_rows * turn),
        total_fade * jnp.sin(n_rows * turn),
        final[1],
        final[2],
    )
    return (outputs, totals)


def per_device(
    resid,
    mix_in,
    decay_rate,
    turn_rate,
    forget,
    input_real,
    input_imag,
    output_real,
    output_imag,
    skip_gain,
    mix_gain,
    w_out,
    ffn_gain,
    gating_matrix,
    w_up,
    w_down,
):
    high = lax.Precision.DEFAULT
    n_rows, local_width = mix_in.shape
    n_groups, n_state = decay_rate.shape
    n_chan = input_real.shape[2]
    full_gate, full_up, full_down = rows_first((gating_matrix, w_up, w_down), "sp", (0, 0, 1))
    drive = mix_in.astype(jnp.float32).reshape(n_rows, n_groups, n_chan)
    in_factor = jnp.sqrt(-jnp.expm1(2.0 * decay_rate))
    push_real = jnp.einsum(
        "gph,tgh->tgp", input_real * in_factor[:, :, None], drive, precision=high
    ).reshape(n_rows, n_groups * n_state)
    push_imag = jnp.einsum(
        "gph,tgh->tgp", input_imag * in_factor[:, :, None], drive, precision=high
    ).reshape(n_rows, n_groups * n_state)
    log_step = (decay_rate[None] + forget[:, :, None]).reshape(n_rows, n_groups * n_state)
    turn = turn_rate.reshape(n_groups * n_state)
    outputs, totals = local_states(log_step, push_real, push_imag, turn)
    inner_real, inner_imag, prefix_real, prefix_imag = outputs
    ones_row = jnp.ones((n_groups * n_state,), jnp.float32)
    zeroed_row = jnp.zeros((n_groups * n_state,), jnp.float32)
    carry_in = entering(totals, "sp", chain, (ones_row, zeroed_row, zeroed_row, zeroed_row))
    state_real = inner_real + prefix_real * carry_in[2][None] - prefix_imag * carry_in[3][None]
    state_imag = inner_imag + prefix_real * carry_in[3][None] + prefix_imag * carry_in[2][None]
    response = (
        jnp.einsum(
            "ghp,tgp->tgh",
            output_real,
            state_real.reshape(n_rows, n_groups, n_state),
            precision=high,
        )
        - jnp.einsum(
            "ghp,tgp->tgh",
            output_imag,
            state_imag.reshape(n_rows, n_groups, n_state),
            precision=high,
        )
        + skip_gain[None] * drive
    )
    mixer_out = jax.nn.gelu(response.reshape(n_rows, local_width)).astype(jnp.bfloat16)
    swapped = lax.all_to_all(mixer_out, "tp", split_axis=0, concat_axis=1, tiled=True)
    mixed_f = swapped.astype(jnp.float32)
    normed = (
        mixed_f * lax.rsqrt(jnp.mean(mixed_f * mixed_f, axis=1, keepdims=True) + eps) * mix_gain
    ).astype(jnp.bfloat16)
    projected = jnp.dot(normed, w_out, preferred_element_type=jnp.float32)
    resid_mid = resid.astype(jnp.float32) + projected
    ffn_in = (
        resid_mid
        * lax.rsqrt(jnp.mean(resid_mid * resid_mid, axis=1, keepdims=True) + eps)
        * ffn_gain
    ).astype(jnp.bfloat16)
    gathered = collect(ffn_in, "tp", 0)
    gate_val = jnp.dot(gathered, full_gate, preferred_element_type=jnp.float32)
    up_val = jnp.dot(gathered, full_up, preferred_element_type=jnp.float32)
    hidden = (jax.nn.silu(gate_val) * up_val).astype(jnp.bfloat16)
    partial_value = jnp.dot(hidden, full_down, preferred_element_type=jnp.float32)
    ffn = sent_and_summed(partial_value.astype(jnp.bfloat16), "tp", 0)
    return (resid_mid + 0.5 * ffn).astype(jnp.bfloat16)


def solution(mesh):
    placed = (
        P(("sp", "tp"), None),
        P("sp", "tp"),
        P("tp", None),
        P("tp", None),
        P("sp", "tp"),
        P("tp", None, None),
        P("tp", None, None),
        P("tp", None, None),
        P("tp", None, None),
        P("tp", None),
        P(),
        P(),
        P(),
        P("sp", "tp"),
        P("sp", "tp"),
        P("tp", "sp"),
    )
    return jax.shard_map(
        per_device, mesh=mesh, in_specs=placed, out_specs=P(("sp", "tp"), None), check_vma=False
    )
```

profile of v0, /device:TPU:1, one launch (start us, length us, event | category | flops | bytes accessed | tf_op | source)
XLA Modules:
  0.0 231.2 jit_solution(3535144816180970547)
XLA Ops:
  6.5 1.9 pad_maximum_fusion
  10.0 0.9 copy.57
  12.4 1.9 convolution_bitcast_fusion.2
  14.3 1.5 copy.58
  15.8 1.1 reshape_reshape.7
  16.9 1.1 convolution_bitcast_fusion.1
  18.0 1.5 copy.59
  19.5 1.1 reshape_reshape.8
  21.0 1.1 add.193
  22.2 1.1 broadcast_add_fusion
  23.3 92.7 %while.29 = (s32[]{:T(128)}, f32[512]{0:T(512)S(1)}, f32[512]{0:T(512)S(1)}, f32[512]{0:T(512)S(1)}, f32[]{:T(128)}, /*index=5*/f32[8,32,512]{2,1,0:T(8,128)}, f...) while((s32[]{:T(128)}, f32[512]{0:T(512)S(1)}, ...), condition=%wide.wide.region_3.4_spmd.clone.clone.clone.clone, body=%wide.wide.region_0.3_spmd.clone.clone.clone.clone.sunk | while | flops 9654340 | bytes 1319007 | solution.py:148
  24.3 9.2 %add_reduce_fusion.3 = (f32[32,512]{1,0:T(8,128)S(1)}, f32[32,512]{1,0:T(8,128)S(1)}) fusion(f32[512]{0:T(512)S(1)} %get-tuple-element.735, f32[32,32]{1,0:T(8,128)S(1)} %get-tuple-element.736, f32[32,512]{1,0:T(8,128)S(1)} %get-tuple-element.670, f32[32,512]{1,0:T(8,128)S(1)} %get-tuple-element.671, ...), kind=kLoop, calls=%fused_computation.13.clone.clone.1 | loop fusion | flops 8355840 | bytes 335872 | tf_op jit(solution)/shard_map/while/body/eval_jaxpr/reduce_sum | solution.py:128
  33.6 1.2 fusion.106
  35.9 9.2 %add_reduce_fusion.3 = (f32[32,512]{1,0:T(8,128)S(1)}, f32[32,512]{1,0:T(8,128)S(1)}) fusion(f32[512]{0:T(512)S(1)} %get-tuple-element.735, f32[32,32]{1,0:T(8,128)S(1)} %get-tuple-element.736, f32[32,512]{1,0:T(8,128)S(1)} %get-tuple-element.670, f32[32,512]{1,0:T(8,128)S(1)} %get-tuple-element.671, ...), kind=kLoop, calls=%fused_computation.13.clone.clone.1 | loop fusion | flops 8355840 | bytes 335872 | tf_op jit(solution)/shard_map/while/body/eval_jaxpr/reduce_sum | solution.py:128
  45.1 1.3 fusion.106
  46.4 0.9 dynamic-slice_bitcast_fusion.4
  47.5 9.2 %add_reduce_fusion.3 = (f32[32,512]{1,0:T(8,128)S(1)}, f32[32,512]{1,0:T(8,128)S(1)}) fusion(f32[512]{0:T(512)S(1)} %get-tuple-element.735, f32[32,32]{1,0:T(8,128)S(1)} %get-tuple-element.736, f32[32,512]{1,0:T(8,128)S(1)} %get-tuple-element.670, f32[32,512]{1,0:T(8,128)S(1)} %get-tuple-element.671, ...), kind=kLoop, calls=%fused_computation.13.clone.clone.1 | loop fusion | flops 8355840 | bytes 335872 | tf_op jit(solution)/shard_map/while/body/eval_jaxpr/reduce_sum | solution.py:128
  56.7 1.3 fusion.106
  59.1 9.2 %add_reduce_fusion.3 = (f32[32,512]{1,0:T(8,128)S(1)}, f32[32,512]{1,0:T(8,128)S(1)}) fusion(f32[512]{0:T(512)S(1)} %get-tuple-element.735, f32[32,32]{1,0:T(8,128)S(1)} %get-tuple-element.736, f32[32,512]{1,0:T(8,128)S(1)} %get-tuple-element.670, f32[32,512]{1,0:T(8,128)S(1)} %get-tuple-element.671, ...), kind=kLoop, calls=%fused_computation.13.clone.clone.1 | loop fusion | flops 8355840 | bytes 335872 | tf_op jit(solution)/shard_map/while/body/eval_jaxpr/reduce_sum | solution.py:128
  68.3 1.3 fusion.106
  70.6 9.2 %add_reduce_fusion.3 = (f32[32,512]{1,0:T(8,128)S(1)}, f32[32,512]{1,0:T(8,128)S(1)}) fusion(f32[512]{0:T(512)S(1)} %get-tuple-element.735, f32[32,32]{1,0:T(8,128)S(1)} %get-tuple-element.736, f32[32,512]{1,0:T(8,128)S(1)} %get-tuple-element.670, f32[32,512]{1,0:T(8,128)S(1)} %get-tuple-element.671, ...), kind=kLoop, calls=%fused_computation.13.clone.clone.1 | loop fusion | flops 8355840 | bytes 335872 | tf_op jit(solution)/shard_map/while/body/eval_jaxpr/reduce_sum | solution.py:128
  79.9 1.3 fusion.106
  82.2 9.2 %add_reduce_fusion.3 = (f32[32,512]{1,0:T(8,128)S(1)}, f32[32,512]{1,0:T(8,128)S(1)}) fusion(f32[512]{0:T(512)S(1)} %get-tuple-element.735, f32[32,32]{1,0:T(8,128)S(1)} %get-tuple-element.736, f32[32,512]{1,0:T(8,128)S(1)} %get-tuple-element.670, f32[32,512]{1,0:T(8,128)S(1)} %get-tuple-element.671, ...), kind=kLoop, calls=%fused_computation.13.clone.clone.1 | loop fusion | flops 8355840 | bytes 335872 | tf_op jit(solution)/shard_map/while/body/eval_jaxpr/reduce_sum | solution.py:128
  91.5 1.3 fusion.106
  92.8 0.9 dynamic-slice_bitcast_fusion.4
  93.9 9.2 %add_reduce_fusion.3 = (f32[32,512]{1,0:T(8,128)S(1)}, f32[32,512]{1,0:T(8,128)S(1)}) fusion(f32[512]{0:T(512)S(1)} %get-tuple-element.735, f32[32,32]{1,0:T(8,128)S(1)} %get-tuple-element.736, f32[32,512]{1,0:T(8,128)S(1)} %get-tuple-element.670, f32[32,512]{1,0:T(8,128)S(1)} %get-tuple-element.671, ...), kind=kLoop, calls=%fused_computation.13.clone.clone.1 | loop fusion | flops 8355840 | bytes 335872 | tf_op jit(solution)/shard_map/while/body/eval_jaxpr/reduce_sum | solution.py:128
  103.1 1.2 fusion.106
  104.4 0.9 dynamic-slice_bitcast_fusion.4
  105.5 9.2 %add_reduce_fusion.3 = (f32[32,512]{1,0:T(8,128)S(1)}, f32[32,512]{1,0:T(8,128)S(1)}) fusion(f32[512]{0:T(512)S(1)} %get-tuple-element.735, f32[32,32]{1,0:T(8,128)S(1)} %get-tuple-element.736, f32[32,512]{1,0:T(8,128)S(1)} %get-tuple-element.670, f32[32,512]{1,0:T(8,128)S(1)} %get-tuple-element.671, ...), kind=kLoop, calls=%fused_computation.13.clone.clone.1 | loop fusion | flops 8355840 | bytes 335872 | tf_op jit(solution)/shard_map/while/body/eval_jaxpr/reduce_sum | solution.py:128
  114.7 1.2 fusion.106
  116.9 13.2 %all-to-all-start = ((f32[64,4,512]{2,1,0:T(4,128)}), f32[64,4,512]{2,1,0:T(4,128)}, u32[]{:S(2)}, u32[]{:S(2)}) async-start(f32[64,4,512]{2,1,0:T(4,128)} %broadcast_in_dim.120), calls=%async_computation | async-start | bytes 1048576 | tf_op jit(solution)/shard_map/all_to_all | solution.py:25
  130.2 1.2 reshape.167
  131.4 2.3 reshape.168
  133.7 2.2 reshape.177
  135.9 2.3 reshape.178
  138.2 9.6 %all-to-all-done = f32[64,4,512]{2,1,0:T(4,128)} async-done(((f32[64,4,512]{2,1,0:T(4,128)}), f32[64,4,512]{2,1,0:T(4,128)}, u32[]{:S(2)}, u32[]{:S(2)}) %all-to-all-start) | async-done | bytes 524320 | tf_op jit(solution)/shard_map/all_to_all | solution.py:25
  147.8 2.3 fusion.84
  150.8 0.9 slice.166
  151.8 1.5 slice.167
  153.3 1.5 slice.169
  154.8 1.5 slice.170
  159.0 1.1 multiply_subtract_fusion.2
  163.0 2.2 multiply_add_fusion.1
  166.1 8.4 %all_to_all.25 = bf16[4,64,128]{2,1,0:T(8,128)(2,1)S(1)} all-to-all(bf16[4,64,128]{2,1,0:T(8,128)(2,1)S(1)} %fusion.67), channel_id=1, replica_groups=mesh['sp'=64,'tp'=4] {'tp'}, dimensions={0} | all-to-all | bytes 131072 | tf_op jit(solution)/shard_map/all_to_all | solution.py:216
  175.5 16.5 %all_to_all.26 = bf16[4,64,2048]{2,1,0:T(8,128)(2,1)} all-to-all(bf16[4,64,2048]{2,1,0:T(8,128)(2,1)S(1)} %broadcast_in_dim.123), channel_id=1, replica_groups=mesh['sp'=64,'tp'=4] {'tp'}, dimensions={0} | all-to-all | bytes 2097152 | tf_op jit(solution)/shard_map/all_to_all | solution.py:25
  192.1 5.9 %fusion.35 = f32[256,1408]{1,0:T(8,128)} fusion(bf16[256,2048]{1,0:T(8,128)(2,1)} %bitcast.106, bf16[2048,4224]{1,0:T(8,128)(2,1)} %all-gather.2.cloned.1.call-done), kind=kOutput, calls=%fused_computation.49 | convolution fusion | flops 1476395008 | bytes 8257536 | tf_op jit(solution)/shard_map/dot_general | solution.py:229
  198.0 9.5 %fusion.43 = bf16[256,2048]{1,0:T(8,128)(2,1)} fusion(bf16[2048,4224]{1,0:T(8,128)(2,1)} %all-gather.2.cloned.1.call-done, bf16[256,2048]{1,0:T(8,128)(2,1)} %bitcast.107, f32[256,1408]{1,0:T(8,128)} %fusion.35), kind=kOutput, calls=%fused_computation.53 | convolution fusion | flops 2955476992 | bytes 15073280 | tf_op jit(solution)/shard_map/dot_general | solution.py:232
  207.5 16.0 %all_to_all.27 = bf16[4,64,2048]{2,1,0:T(8,128)(2,1)S(1)} all-to-all(bf16[4,64,2048]{2,1,0:T(8,128)(2,1)} %bitcast.108), channel_id=1, replica_groups=mesh['sp'=64,'tp'=4] {'tp'}, dimensions={0} | all-to-all | bytes 2097152 | tf_op jit(solution)/shard_map/all_to_all | solution.py:88
  (160 shorter events, 19.3 us)
Async XLA Ops:
  6.5 168.1 %copy-start = (bf16[512,2048]{1,0:T(8,128)(2,1)S(1)}, bf16[512,2048]{1,0:T(8,128)(2,1)}, u32[]{:S(2)}) copy-start(bf16[512,2048]{1,0:T(8,128)(2,1)} %param.29) | copy-start | bytes 6291460
  6.5 185.5 %all-gather.2.cloned.1.call-start = ((), (), s32[]{:S(2)}) async-start(), calls=%async_computation.4 | async-start | bytes 17571840 | tf_op jit(solution)/shard_map/all_gather | solution.py:13
  8.4 8.5 %copy-start.3 = (f32[8,64,16]{1,2,0:T(8,128)S(1)}, f32[8,64,16]{1,2,0:T(8,128)}, u32[]{:S(2)}) copy-start(f32[8,64,16]{1,2,0:T(8,128)} %param.24) | copy-start | bytes 98308
  16.9 3.7 %copy-start.5 = (f32[256,8]{0,1:T(8,128)S(1)}, f32[256,8]{0,1:T(8,128)}, u32[]{:S(2)}) copy-start(f32[256,8]{0,1:T(8,128)} %param.22) | copy-start | bytes 24580
  116.9 30.9 %all-to-all-start = ((f32[64,4,512]{2,1,0:T(4,128)}), f32[64,4,512]{2,1,0:T(4,128)}, u32[]{:S(2)}, u32[]{:S(2)}) async-start(f32[64,4,512]{2,1,0:T(4,128)} %broadcast_in_dim.120), calls=%async_computation | async-start | bytes 1048576 | tf_op jit(solution)/shard_map/all_to_all | solution.py:25
  163.0 2.3 copy-start.8
  163.0 2.5 %copy-start.2 = (f32[8,16,64]{2,1,0:T(8,128)S(1)}, f32[8,16,64]{2,1,0:T(8,128)}, u32[]{:S(2)}) copy-start(f32[8,16,64]{2,1,0:T(8,128)} %param.26) | copy-start | bytes 98308
  163.0 2.5 %copy-start.6 = (f32[8,16]{1,0:T(8,128)S(1)}, f32[8,16]{1,0:T(8,128)}, u32[]{:S(2)}) copy-start(f32[8,16]{1,0:T(8,128)} %param.27) | copy-start | bytes 1540
  165.2 9.4 %copy-start.1 = (bf16[64,2048]{1,0:T(8,128)(2,1)S(1)}, bf16[64,2048]{1,0:T(8,128)(2,1)}, u32[]{:S(2)}) copy-start(bf16[64,2048]{1,0:T(8,128)(2,1)} %param.18) | copy-start | bytes 786436
  165.2 9.4 %copy-start.7 = (f32[512]{0:T(512)S(1)}, f32[512]{0:T(512)}, u32[]{:S(2)}) copy-start(f32[512]{0:T(512)} %param.28) | copy-start | bytes 6148
  165.8 9.5 %copy-start.4 = (f32[2048]{0:T(1024)S(1)}, f32[2048]{0:T(1024)}, u32[]{:S(2)}) copy-start(f32[2048]{0:T(1024)} %param.30) | copy-start | bytes 24580
Sparse Core Ops, SparseCore 0:
  10.1 104.7 all-gather.1
where the time goes:
time: 234 us; the launch traced here: 231 us
  other arithmetic  93.8 us (40%)
  blocking collectives  40.9 us (17%)
  local copies, waits for them, and re-layouts  38.8 us (17%)
  matrix products  20.6 us (9%)
  between operations  13.7 us (6%)
  starting transfers between devices  13.3 us (6%)
  waiting for transfers between devices  9.62 us (4%)
    reduce_sum x8, other arithmetic, advance(): jnp.sum(weight_real * imag_block[None] + weight_imag * real_block[None],...  73.5 us
    all_to_all x1, blocking collectives, sent_to_all(): lax.all_to_all(jnp.broadcast_to(value[None], (length, *value.shape)), axi...  16.5 us
    all_to_all x1, blocking collectives, sent_and_summed(): lax.all_to_all(tiles, axis, split_axis=0, concat_axis=0, tiled=True)  16 us
    all_to_all x1, starting transfers between devices, sent_to_all(): lax.all_to_all(jnp.broadcast_to(value[None], (length, *value.shape)), axi...  13.2 us
    dynamic_update_slice x8, other arithmetic, local_states(): final, outputs = lax.scan(advance, start, blocks)  10.1 us
    slice x40, local copies, waits for them, and re-layouts, joined_by_halves(): part[side::2]  9.96 us
    all_to_all x1, waiting for transfers between devices, sent_to_all(): lax.all_to_all(jnp.broadcast_to(value[None], (length, *value.shape)), axi...  9.6 us
    dot_general x1, matrix products, per_device(): jnp.dot(hidden, full_down, preferred_element_type=jnp.float32)  9.48 us
  transfers between devices with their start and end apart: 2, of which 1 were waited for; matrix products, arithmetic and copies ran while one was open for 58% of the time, Pallas kernels for 0%

commit v1 on v0

v1 whole, which is shorter than its diff:
```python
import functools

import jax
import jax.numpy as jnp
from jax import lax
from jax.experimental import pallas as pl
from jax.experimental.pallas import tpu as pltpu
from jax.sharding import PartitionSpec as P

f32, bf16 = jnp.float32, jnp.bfloat16
HIGH = lax.Precision.HIGHEST
MESH = pl.DeviceIdType.MESH
eps = 1e-06
NZ, NY, NC, NX = 8, 4, 2, 4
ROWS = 256
GROUPS, CHAN, STATE = 8, 16, 64
LANES = 2 * STATE
WIDE = GROUPS * LANES
LOCAL = GROUPS * CHAN
D, HID, SHARD = 2048, 1408, 32
OWN = ROWS // NX
PATH_A, PATH_A1, PATH_A2 = (0, 512), (0, 256), (256, 512)
PATH_B, PATH_B1, PATH_B2 = (512, 1408), (512, 896), (896, 1408)
PHASES = ((0, 2), (2, 1))
PLANES = (0, -1, 1, -2, 2, -3, 3, 4)
ORDER = (
    "0a0", "0b0", "local", "c1", "0s0", "0y0", "r0", "masked", "outmap", "1b0", "0a1", "0s1", "1a0", "0b1",
    "0y1", "carry", "c2", "0q01", "0f0", "0s2", "0y2", "0q11", "r1", "0q31", "0f1", "0d0", "1a1", "0b2",
    "0y3", "0e0", "r2", "0f2", "0q02", "0y4", "far", "resp", "m", "0q21", "0q12", "0d1", "0f3", "0q32",
    "0d2", "1y0", "0e1", "0e2", "0b3", "0y5", "0q03", "0f4", "0q22", "0d3", "0y6", "proj", "0q13", "first0",
    "0e3", "first1", "0q33", "0f5", "first2", "first3", "0b4", "0d4", "0y7", "1b1", "0q04", "1s0", "0e4",
    "first4", "0q23", "0q34", "0f6", "1s1", "0d5", "0q14", "1f0", "1s2", "1y1", "1b2", "0e5", "first5",
    "0f7", "0q24", "1q01", "0d6", "1q11", "1y2", "1d0", "1q31", "1q21", "1y3", "0e6", "first6", "1b3",
    "1e0", "1f1", "1q02", "0d7", "1y4", "1q12", "1q32", "1f2", "1q22", "1y5", "0e7", "first7", "hidden",
    "1b4", "second0", "scat0", "1q03", "1d1", "1f3", "1q13", "1y6", "1q33", "1d2", "1f4", "1e1", "second1",
    "scat1", "1q23", "1y7", "1q04", "1e2", "second2", "scat2", "1q14", "1d3", "1f5", "1q34", "fin0", "1f6",
    "1q24", "1e3", "second3", "scat3", "1d4", "fin1", "1f7", "1d5", "1e4", "second4", "scat4", "1d6",
    "fin2", "1e5", "second5", "scat5", "1d7", "1e6", "second6", "scat6", "fin3", "1e7", "second7", "scat7",
    "fin4", "fin5", "fin6", "fin7",
)


def iota(shape, dim):
    return lax.broadcasted_iota(jnp.int32, shape, dim)


def where_one(test):
    return jnp.where(test, 1.0, 0.0).astype(f32)


def nt(a, b, precision=None):
    return lax.dot_general(
        a, b, (((1,), (1,)), ((), ())), precision=precision, preferred_element_type=f32
    )


def nn(a, b, precision=None):
    return lax.dot_general(
        a, b, (((1,), (0,)), ((), ())), precision=precision, preferred_element_type=f32
    )


def swap(a):
    return pltpu.roll(a, STATE, 1)


def sign_lanes(shape):
    return jnp.where(iota(shape, 1) < STATE, -1.0, 1.0).astype(f32)


def turned(a, c, s):
    return a * c + swap(a) * s


def silu(x):
    return x * jax.nn.sigmoid(x)


def kernel(
    resid, mix, forget_t, decay, turn, in_re, in_im, out_re, out_im, skip, mix_gain, w_out, ffn_gain,
    gate, up, down_t, out,
    G, RA, WO, MX, X, RM, GA, UA, HB, PT, RS, UB, YB, ST, C1, C2,
    send_sem, recv_sem, local_sem,
):
    me, x = lax.axis_index("sp"), lax.axis_index("tp")
    c = lax.rem(me, NC)
    y = lax.rem(lax.div(me, NC), NY)
    z = lax.div(me, NC * NY)
    slot = lax.rem(me, NC * NY)

    def at_sp(zz, yy, cc):
        return {"sp": (zz * NY + yy) * NC + cc}

    def zr(d):
        return lax.rem(z + (d + NZ), NZ)

    def yr(d):
        return lax.rem(y + (d + NY), NY)

    def xr(d):
        return lax.rem(x + (d + NX), NX)

    plane_peers = [{"sp": z * NY * NC + lax.rem(slot + d, NY * NC)} for d in range(1, NY * NC)]
    z_peers = [at_sp(zr(d), y, c) for d in range(1, NZ)]
    x_peers = [{"tp": xr(d)} for d in range(1, NX)]
    yp, ym = at_sp(z, yr(1), c), at_sp(z, yr(-1), c)
    zp, zm = at_sp(zr(1), y, c), at_sp(zr(-1), y, c)
    partner = at_sp(z, y, 1 - c)

    numbers, pending = {}, []

    def number(name):
        return numbers.setdefault(name, len(numbers))

    def send(name, src, dst, to):
        k = number(name)
        copy = pltpu.make_async_remote_copy(
            src_ref=src, dst_ref=dst, send_sem=send_sem.at[k], recv_sem=recv_sem.at[k],
            device_id=to, device_id_type=MESH,
        )
        copy.start()
        pending.append(copy)

    def recv(name, dst):
        k = number(name)
        pltpu.make_async_remote_copy(
            src_ref=dst, dst_ref=dst, send_sem=send_sem.at[k], recv_sem=recv_sem.at[k],
            device_id=partner, device_id_type=MESH,
        ).wait_recv()

    tasks = {}

    def task(f):
        tasks[f.__name__] = f
        return f

    def block(p, dz, dy, lanes):
        first, count = PHASES[p]
        return G.at[
            pl.ds(first, count), zr(dz), yr(dy), c, :, pl.ds(lanes[0], lanes[1] - lanes[0])
        ]

    def gather_tasks(p):
        first, count = PHASES[p]

        def go(name, ref, to):
            send(f"{p}{name}", ref, ref, to)

        def got(name, ref):
            recv(f"{p}{name}", ref)

        def both(name, ref, plus, minus):
            go(name + "+", ref, plus)
            go(name + "-", ref, minus)

        def a0():
            both("A0", block(p, 0, 0, PATH_A), yp, ym)

        def b0():
            both("B1", block(p, 0, 0, PATH_B), zp, zm)

        def a1():
            got("A0+", block(p, 0, -1, PATH_A))
            go("A1+", block(p, 0, -1, PATH_A1), yp)
            got("A0-", block(p, 0, 1, PATH_A))
            go("A1-", block(p, 0, 1, PATH_A2), ym)

        def s0():
            both("Z01", block(p, 0, 0, PATH_A), zp, zm)

        def s1():
            both("Z11", block(p, 0, -1, PATH_A), zp, zm)
            both("Z31", block(p, 0, 1, PATH_A), zp, zm)

        def s2():
            got("A1+", block(p, 0, -2, PATH_A1))
            got("A1-", block(p, 0, 2, PATH_A2))
            both("Z21", block(p, 0, 2, PATH_A), zp, zm)

        def q(row, s):
            dy = (0, -1, 2, 1)[row]
            if s < 4 or row in (0, 1):
                got(f"Z{row}{s}+", block(p, -s, dy, PATH_A))
                if s < 3 or (s == 3 and row in (0, 1)):
                    go(f"Z{row}{s + 1}+", block(p, -s, dy, PATH_A), zp)
            if s < 4 or row in (2, 3):
                got(f"Z{row}{s}-", block(p, s, dy, PATH_A))
                if s < 3 or (s == 3 and row in (2, 3)):
                    go(f"Z{row}{s + 1}-", block(p, s, dy, PATH_A), zm)

        def b(s):
            got(f"B{s}+", block(p, -s, 0, PATH_B if s < 4 else PATH_B1))
            if s < 4:
                go(f"B{s + 1}+", block(p, -s, 0, PATH_B if s < 3 else PATH_B1), zp)
            got(f"B{s}-", block(p, s, 0, PATH_B if s < 4 else PATH_B2))
            if s < 4:
                go(f"B{s + 1}-", block(p, s, 0, PATH_B if s < 3 else PATH_B2), zm)

        def y_(k):
            both(f"Y{k}", block(p, PLANES[k], 0, PATH_B), yp, ym)

        def f(k):
            got(f"Y{k}+", block(p, PLANES[k], -1, PATH_B))
            go(f"F{k}+", block(p, PLANES[k], -1, PATH_B1), yp)
            got(f"Y{k}-", block(p, PLANES[k], 1, PATH_B))
            go(f"F{k}-", block(p, PLANES[k], 1, PATH_B2), ym)

        def d(k):
            got(f"F{k}+", block(p, PLANES[k], -2, PATH_B1))
            got(f"F{k}-", block(p, PLANES[k], 2, PATH_B2))
            go(f"D{k}", G.at[pl.ds(first, count), zr(PLANES[k]), :, c], partner)

        def e(k):
            got(f"D{k}", G.at[pl.ds(first, count), zr(PLANES[k]), :, 1 - c])

        for name, f_ in (("a0", a0), ("b0", b0), ("a1", a1), ("s0", s0), ("s1", s1), ("s2", s2)):
            tasks[f"{p}{name}"] = f_
        for s in range(1, 5):
            tasks[f"{p}b{s}"] = functools.partial(b, s)
            for row in range(NY):
                tasks[f"{p}q{row}{s}"] = functools.partial(q, row, s)
        for k in range(NZ):
            tasks[f"{p}y{k}"] = functools.partial(y_, k)
            tasks[f"{p}f{k}"] = functools.partial(f, k)
            tasks[f"{p}d{k}"] = functools.partial(d, k)
            tasks[f"{p}e{k}"] = functools.partial(e, k)

    for p in range(len(PHASES)):
        gather_tasks(p)

    loads = [
        pltpu.make_async_copy(gate, G.at[0, z, y, c], local_sem.at[0]),
        pltpu.make_async_copy(up, G.at[1, z, y, c], local_sem.at[1]),
        pltpu.make_async_copy(down_t, G.at[2, z, y, c], local_sem.at[2]),
        pltpu.make_async_copy(resid, RA.at[x], local_sem.at[3]),
        pltpu.make_async_copy(w_out, WO, local_sem.at[4]),
    ]
    for load in loads:
        load.start()
    barrier = pltpu.get_barrier_semaphore()
    peers = plane_peers + z_peers + x_peers
    for peer in peers:
        pl.semaphore_signal(barrier, inc=1, device_id=peer, device_id_type=MESH)

    with jax.named_scope("prep"):
        drive = mix[...]
        spread = where_one(lax.rem(iota((CHAN, LOCAL), 1), CHAN) == iota((CHAN, LOCAL), 0))
        twice = where_one(lax.rem(iota((STATE, LANES), 1), STATE) == iota((STATE, LANES), 0))
        rate2 = nn(decay[...], twice, HIGH)
        turn2 = nn(turn[...], twice, HIGH)
        lower = iota((ROWS, ROWS), 0) >= iota((ROWS, ROWS), 1)
        lower_one = where_one(lower)
        forget_rows = forget_t[...]
        run_log = nt(lower_one, forget_rows, HIGH)
        run_log_t = nt(forget_rows, lower_one, HIGH)
        w = 2.0 * rate2
        series = 1.0 + w / 6.0
        for k in (5.0, 4.0, 3.0, 2.0):
            series = 1.0 + (w / k) * series
        in_factor = jnp.sqrt(-(w * series))
        first_half = where_one(iota((STATE, LANES), 1) == iota((STATE, LANES), 0)).astype(bf16)
        second_half = where_one(
            iota((STATE, LANES), 1) == iota((STATE, LANES), 0) + STATE
        ).astype(bf16)
        row_group = lax.div(iota((LOCAL, LANES), 0), CHAN)

        def by_group(rows):
            return jnp.concatenate(
                [jnp.where(row_group == g, rows, 0.0).astype(bf16) for g in range(GROUPS)], axis=1
            )

        in_map = by_group(
            nn(in_re[...].astype(bf16), first_half) + nn(in_im[...].astype(bf16), second_half)
        )
        UB[...] = nn(drive, in_map)
        sign = sign_lanes((1, LANES))
        sign8 = sign_lanes((GROUPS, LANES))
        coarse = (iota((16, LANES), 0) - 8).astype(f32) * 16.0
        fine = iota((16, LANES), 0).astype(f32)
        centred = (iota((ROWS, LANES), 0) - ROWS // 2).astype(f32)
    with jax.named_scope("entry"):
        pl.semaphore_wait(barrier, len(peers))
        for load in loads[:3]:
            load.wait()

    def phase_tables(g):
        angle = turn2[g : g + 1]
        ca, sa = jnp.cos(angle * coarse), jnp.sin(angle * coarse)
        cb, sb = jnp.cos(angle * fine), jnp.sin(angle * fine)
        cos = [ca[k : k + 1] * cb - sa[k : k + 1] * sb for k in range(16)]
        sin = [sa[k : k + 1] * cb + ca[k : k + 1] * sb for k in range(16)]
        return jnp.concatenate(cos, axis=0), jnp.concatenate(sin, axis=0) * sign

    def power(n, log=0.0):
        size = jnp.exp(rate2 * n + log)
        return size * jnp.cos(turn2 * n), size * jnp.sin(turn2 * n) * sign8

    v = {}

    @task
    def local():
        ends = []
        last = run_log[ROWS - 1 : ROWS]
        for g in range(GROUPS):
            lanes = slice(LANES * g, LANES * (g + 1))
            cos, sin = phase_tables(g)
            grow = jnp.exp(-rate2[g : g + 1] * centred) * in_factor[g : g + 1]
            b_g = UB[:, lanes]
            u = (b_g * cos - swap(b_g) * sin) * grow
            UB[:, lanes] = u
            fall = jnp.exp(rate2[g : g + 1] * centred)
            ST[0, :, lanes] = cos * fall
            ST[1, :, lanes] = sin * fall
            weight = jnp.exp(last[:, g : g + 1] - run_log[:, g : g + 1])
            total = jnp.sum(u * weight, axis=0, keepdims=True)
            at_end = slice(ROWS - 1, ROWS)
            ends.append(turned(total, ST[0, at_end, lanes], ST[1, at_end, lanes]))
        last_col = jnp.sum(
            jnp.where(iota((GROUPS, ROWS), 1) == ROWS - 1, run_log_t, 0.0), axis=1, keepdims=True
        )
        C1[slot, 0:GROUPS] = jnp.concatenate(ends, axis=0)
        C1[slot, GROUPS:] = jnp.broadcast_to(last_col, (GROUPS, LANES))

    @task
    def c1():
        for d in range(1, NY * NC):
            send(f"C1{d}", C1.at[slot], C1.at[slot], plane_peers[d - 1])

    @task
    def masked():
        for g in range(GROUPS):
            lanes = slice(LANES * g, LANES * (g + 1))
            gap = run_log[:, g : g + 1] - run_log_t[g : g + 1]
            weights = jnp.where(lower, jnp.exp(jnp.minimum(gap, 0.0)), 0.0).astype(bf16)
            YB[:, lanes] = nn(weights, UB[:, lanes].astype(bf16))

    @task
    def carry():
        c_one, s_one = power(float(ROWS))
        for d in range(1, NY * NC):
            recv(f"C1{d}", C1.at[lax.rem(slot - d + NY * NC, NY * NC)])
        acc = jnp.zeros((GROUPS, LANES), f32)
        log_acc = jnp.zeros((GROUPS, LANES), f32)
        before, log_before = acc, log_acc
        for j in range(NY * NC):
            here = slot == j
            before = jnp.where(here, acc, before)
            log_before = jnp.where(here, log_acc, log_before)
            log_j = C1[j, GROUPS:]
            acc = jnp.exp(log_j) * turned(acc, c_one, s_one) + C1[j, 0:GROUPS]
            log_acc = log_acc + log_j
        C2[z, 0:GROUPS] = acc
        C2[z, GROUPS:] = log_acc
        v["before"], v["log_before"] = before, log_before

    @task
    def c2():
        for d in range(1, NZ):
            send(f"C2{d}", C2.at[z], C2.at[z], z_peers[d - 1])

    @task
    def outmap():
        v["out_map"] = by_group(
            nn(out_re[...].astype(bf16), first_half) - nn(out_im[...].astype(bf16), second_half)
        )
        skip_rows = nn(skip[...], spread, HIGH)
        in_group = lax.div(iota((GROUPS, LOCAL), 1), CHAN) == iota((GROUPS, LOCAL), 0)
        v["skip_row"] = jnp.sum(jnp.where(in_group, skip_rows, 0.0), axis=0, keepdims=True)

    @task
    def far():
        c_plane, s_plane = power(float(ROWS * NY * NC))
        c_in, s_in = power(slot.astype(f32) * float(ROWS), v["log_before"])
        c_mid, s_mid = power(float(ROWS // 2 + 1))
        for d in range(1, NZ):
            recv(f"C2{d}", C2.at[zr(-d)])
        total = jnp.zeros((GROUPS, LANES), f32)
        for j in range(NZ):
            step_on = jnp.exp(C2[j, GROUPS:]) * turned(total, c_plane, s_plane) + C2[j, 0:GROUPS]
            total = jnp.where(j < z, step_on, total)
        v["carry"] = turned(v["before"] + turned(total, c_in, s_in), c_mid, s_mid)

    @task
    def resp():
        for g in range(GROUPS):
            lanes = slice(LANES * g, LANES * (g + 1))
            full = YB[:, lanes] + jnp.exp(run_log[:, g : g + 1]) * v["carry"][g : g + 1]
            YB[:, lanes] = turned(full, ST[0, :, lanes], ST[1, :, lanes])
        response = nt(YB[...].astype(bf16), v["out_map"]) + v["skip_row"] * drive.astype(f32)
        MX[x] = jax.nn.gelu(response).astype(bf16)

    @task
    def m():
        for d in range(1, NX):
            send(f"M{d}", MX.at[x], MX.at[x], x_peers[d - 1])

    half = OWN // 2

    @task
    def r0():
        loads[3].wait()
        send("R+", RA.at[x], RA.at[x], x_peers[0])
        send("R-", RA.at[x], RA.at[x], x_peers[2])

    @task
    def r1():
        recv("R+", RA.at[xr(-1)])
        send("Q+", RA.at[xr(-1), 0:half], RA.at[xr(-1), 0:half], x_peers[0])
        recv("R-", RA.at[xr(1)])
        send("Q-", RA.at[xr(1), half:], RA.at[xr(1), half:], x_peers[2])

    @task
    def r2():
        recv("Q+", RA.at[xr(-2), 0:half])
        recv("Q-", RA.at[xr(2), half:])
        loads[4].wait()

    @task
    def proj():
        for d in range(1, NX):
            recv(f"M{d}", MX.at[xr(-d)])
        mixed = [MX[q].astype(f32) for q in range(NX)]
        total = sum(jnp.sum(m * m, axis=1, keepdims=True) for m in mixed)
        scale = lax.rsqrt(total / float(LOCAL * NX) + eps)
        gains = mix_gain[...]
        normed = jnp.concatenate(
            [
                (mixed[q] * scale * gains[:, LOCAL * q : LOCAL * (q + 1)]).astype(bf16)
                for q in range(NX)
            ],
            axis=1,
        )
        squares = jnp.zeros((ROWS, 1), f32)
        for k in range(4):
            lanes = slice(512 * k, 512 * (k + 1))
            piece = nn(normed, WO[:, lanes]) + RA[:, :, lanes].reshape(ROWS, 512).astype(f32)
            RM[:, lanes] = piece
            squares = squares + jnp.sum(piece * piece, axis=1, keepdims=True)
        scale = lax.rsqrt(squares / float(D) + eps)
        for k in range(4):
            lanes = slice(512 * k, 512 * (k + 1))
            X[:, lanes] = (RM[:, lanes] * scale * ffn_gain[:, lanes]).astype(bf16)

    def column_slice(k):
        return pl.ds(pl.multiple_of(zr(PLANES[k]) * ROWS, ROWS), ROWS)

    def first(k):
        piece = X[:, column_slice(k)]
        for m, store in ((0, GA), (1, UA)):
            product = nn(piece, G[m, zr(PLANES[k])].reshape(ROWS, HID))
            store[...] = product if k == 0 else store[...] + product

    @task
    def hidden():
        HB[...] = (silu(GA[...]) * UA[...]).astype(bf16)

    def second(k):
        part = nt(HB[...], G[2, zr(PLANES[k])].reshape(ROWS, HID))
        PT[:, :, column_slice(k)] = part.astype(bf16).reshape(NX, OWN, ROWS)

    def scat(k):
        cols = column_slice(k)
        for d in range(1, NX):
            send(f"S{k}{d}", PT.at[xr(d), :, cols], RS.at[x, :, cols], x_peers[d - 1])

    def fin(k):
        cols = column_slice(k)
        ffn = PT[x, :, cols].astype(f32)
        for d in range(1, NX):
            recv(f"S{k}{d}", RS.at[xr(-d), :, cols])
            ffn = ffn + RS[xr(-d), :, cols].astype(f32)
        kept = RM[pl.ds(pl.multiple_of(x * OWN, OWN), OWN), cols]
        out[:, cols] = (kept + 0.5 * ffn).astype(bf16)

    for k in range(NZ):
        tasks[f"first{k}"] = functools.partial(first, k)
        tasks[f"second{k}"] = functools.partial(second, k)
        tasks[f"scat{k}"] = functools.partial(scat, k)
        tasks[f"fin{k}"] = functools.partial(fin, k)

    for name in ORDER:
        with jax.named_scope(name):
            tasks[name]()
    with jax.named_scope("drain"):
        for copy in pending:
            copy.wait_send()


def per_device(
    resid, mix_in, decay_rate, turn_rate, forget, input_real, input_imag, output_real, output_imag,
    skip_gain, mix_gain, w_out, ffn_gain, gating_matrix, w_up, w_down,
):
    vmem = pl.BlockSpec(memory_space=pltpu.VMEM)
    anywhere = pl.BlockSpec(memory_space=pl.ANY)
    n_sems = 256
    return pl.pallas_call(
        kernel,
        out_shape=jax.ShapeDtypeStruct((OWN, D), bf16),
        in_specs=[anywhere] + [vmem] * 10 + [anywhere, vmem] + [anywhere] * 3,
        out_specs=vmem,
        scratch_shapes=[
            pltpu.VMEM((3, NZ, NY, NC, SHARD, HID), bf16),
            pltpu.VMEM((NX, OWN, D), bf16),
            pltpu.VMEM((LOCAL * NX, D), bf16),
            pltpu.VMEM((NX, ROWS, LOCAL), bf16),
            pltpu.VMEM((ROWS, D), bf16),
            pltpu.VMEM((ROWS, D), f32),
            pltpu.VMEM((ROWS, HID), f32),
            pltpu.VMEM((ROWS, HID), f32),
            pltpu.VMEM((ROWS, HID), bf16),
            pltpu.VMEM((NX, OWN, D), bf16),
            pltpu.VMEM((NX, OWN, D), bf16),
            pltpu.VMEM((ROWS, WIDE), f32),
            pltpu.VMEM((ROWS, WIDE), f32),
            pltpu.VMEM((2, ROWS, WIDE), f32),
            pltpu.VMEM((NY * NC, 2 * GROUPS, LANES), f32),
            pltpu.VMEM((NZ, 2 * GROUPS, LANES), f32),
            pltpu.SemaphoreType.DMA((n_sems,)),
            pltpu.SemaphoreType.DMA((n_sems,)),
            pltpu.SemaphoreType.DMA((5,)),
        ],
        compiler_params=pltpu.CompilerParams(
            collective_id=0, has_side_effects=True, vmem_limit_bytes=60 * 1024 * 1024
        ),
    )(
        resid, mix_in, forget.T, decay_rate, turn_rate,
        input_real.transpose(0, 2, 1).reshape(-1, STATE),
        input_imag.transpose(0, 2, 1).reshape(-1, STATE),
        output_real.reshape(-1, STATE), output_imag.reshape(-1, STATE),
        skip_gain, mix_gain.reshape(1, -1), w_out, ffn_gain.reshape(1, -1),
        gating_matrix, w_up, w_down.T,
    )


def solution(mesh):
    placed = (
        P(("sp", "tp"), None),
        P("sp", "tp"),
        P("tp", None),
        P("tp", None),
        P("sp", "tp"),
        P("tp", None, None),
        P("tp", None, None),
        P("tp", None, None),
        P("tp", None, None),
        P("tp", None),
        P(),
        P(),
        P(),
        P("sp", "tp"),
        P("sp", "tp"),
        P("tp", "sp"),
    )
    return jax.shard_map(
        per_device, mesh=mesh, in_specs=placed, out_specs=P(("sp", "tp"), None), check_vma=False
    )
```

time: 234 us -> 79.8 us (0.34); the launches traced: 231 us -> 79.7 us
  other arithmetic: 93.8 us -> 0 us
  Pallas kernels: 0 us -> 78 us
  blocking collectives: 40.9 us -> 0 us
  local copies, waits for them, and re-layouts: 38.8 us -> 1.67 us
  matrix products: 20.6 us -> 0 us
  between operations: 13.7 us -> 0.01 us
  starting transfers between devices: 13.3 us -> 0 us
  waiting for transfers between devices: 9.62 us -> 0 us
    pallas_call x0 -> x1, Pallas kernels: none -> 78 us  [per_device(): pl.pallas_call(kernel, out_shape=jax.ShapeDtypeStruct((OWN, D), bf16), in...]
    reduce_sum x10 -> x0, other arithmetic: 73.8 us -> none  [the longest x8 73.5 us: advance(): jnp.sum(weight_real * imag_block[None] + weight_imag * real_block[None],...]
    all_to_all x3 -> x0, blocking collectives: 40.9 us -> none  [the longest x1 16.5 us: sent_to_all(): lax.all_to_all(jnp.broadcast_to(value[None], (length, *value.shape)), axi...]
    dot_general x15 -> x0, matrix products: 20.6 us -> none  [the longest x1 9.48 us: per_device(): jnp.dot(hidden, full_down, preferred_element_type=jnp.float32)]
    all_to_all x1 -> x0, starting transfers between devices: 13.2 us -> none  [sent_to_all(): lax.all_to_all(jnp.broadcast_to(value[None], (length, *value.shape)), axi...]
    slice x65 -> x0, local copies, waits for them, and re-layouts: 12.3 us -> none  [the longest x40 9.96 us: joined_by_halves(): part[side::2]]
    dynamic_update_slice x8 -> x0, other arithmetic: 10.1 us -> none  [local_states(): final, outputs = lax.scan(advance, start, blocks)]
    all_to_all x1 -> x0, waiting for transfers between devices: 9.6 us -> none  [sent_to_all(): lax.all_to_all(jnp.broadcast_to(value[None], (length, *value.shape)), axi...]
  transfers between devices with their start and end apart: 2 -> 0, of which waited for: 1 -> 0; matrix products, arithmetic and copies ran while one was open for 58% -> 0% of each run, Pallas kernels for 0% -> 0%
where the time goes in v1:
time: 79.8 us; the launch traced here: 79.7 us
  Pallas kernels  78 us (98%)
  local copies, waits for them, and re-layouts  1.67 us (2%)
    pallas_call x1, Pallas kernels, per_device(): pl.pallas_call(kernel, out_shape=jax.ShapeDtypeStruct((OWN, D), bf16), in...  78 us
    unnamed x1, local copies, waits for them, and re-layouts  1.67 us

profile of v1, /device:TPU:1, one launch (start us, length us, event | category | flops | bytes accessed | tf_op | source)
XLA Modules:
  0.0 79.7 jit_solution(1611234053496516808)
XLA Ops:
  0.0 78.0 %shard_map.154 = bf16[64,2048]{1,0:T(8,128)(2,1)} custom-call(bf16[64,2048]{1,0:T(8,128)(2,1)} %resid.1, bf16[256,128]{1,0:T(8,128)(2,1)} %mix.1, f32[8,256]{1,0:T(8,128)} %bitcast.17, f32[8,64]{1,0:T(8,128)} %decay.1, f32[8,64]{1,0:T(8,128)} %turn.1, f32[128,64]{1,0:T(8,128)} %bitcast.13, f32[128,64]{1,0:T(8,128)} %bitcast.14, f32[128,64]{1,0:T(8,128)} %bitcast.15, ...), custom_call_target="tpu_custom_call" | custom-call | tf_op jit(solution)/shard_map/pallas_call | solution.py:496
  78.0 1.7 %copy.18 = bf16[64,2048]{1,0:T(8,128)(2,1)} copy(bf16[64,2048]{1,0:T(8,128)(2,1)} %shard_map.154) | data formatting | bytes 524288

commit v2 on v1

--- a/solution.py
+++ b/solution.py
@@ -19,24 +19,25 @@
 LOCAL = GROUPS * CHAN
 D, HID, SHARD = 2048, 1408, 32
 OWN = ROWS // NX
-PATH_A, PATH_A1, PATH_A2 = (0, 512), (0, 256), (256, 512)
-PATH_B, PATH_B1, PATH_B2 = (512, 1408), (512, 896), (896, 1408)
+PATH_A = ((512, 256), (640, 384))
 PHASES = ((0, 2), (2, 1))
 PLANES = (0, -1, 1, -2, 2, -3, 3, 4)
+OPENING = ("0a0", "0b0",)
+N_GROUPS, N_ARRIVALS = 19, 113
 ORDER = (
-    "0a0", "0b0", "local", "c1", "0s0", "0y0", "r0", "masked", "outmap", "1b0", "0a1", "0s1", "1a0", "0b1",
-    "0y1", "carry", "c2", "0q01", "0f0", "0s2", "0y2", "0q11", "r1", "0q31", "0f1", "0d0", "1a1", "0b2",
-    "0y3", "0e0", "r2", "0f2", "0q02", "0y4", "far", "resp", "m", "0q21", "0q12", "0d1", "0f3", "0q32",
-    "0d2", "1y0", "0e1", "0e2", "0b3", "0y5", "0q03", "0f4", "0q22", "0d3", "0y6", "proj", "0q13", "first0",
-    "0e3", "first1", "0q33", "0f5", "first2", "first3", "0b4", "0d4", "0y7", "1b1", "0q04", "1s0", "0e4",
-    "first4", "0q23", "0q34", "0f6", "1s1", "0d5", "0q14", "1f0", "1s2", "1y1", "1b2", "0e5", "first5",
-    "0f7", "0q24", "1q01", "0d6", "1q11", "1y2", "1d0", "1q31", "1q21", "1y3", "0e6", "first6", "1b3",
-    "1e0", "1f1", "1q02", "0d7", "1y4", "1q12", "1q32", "1f2", "1q22", "1y5", "0e7", "first7", "hidden",
-    "1b4", "second0", "scat0", "1q03", "1d1", "1f3", "1q13", "1y6", "1q33", "1d2", "1f4", "1e1", "second1",
-    "scat1", "1q23", "1y7", "1q04", "1e2", "second2", "scat2", "1q14", "1d3", "1f5", "1q34", "fin0", "1f6",
-    "1q24", "1e3", "second3", "scat3", "1d4", "fin1", "1f7", "1d5", "1e4", "second4", "scat4", "1d6",
-    "fin2", "1e5", "second5", "scat5", "1d7", "1e6", "second6", "scat6", "fin3", "1e7", "second7", "scat7",
-    "fin4", "fin5", "fin6", "fin7",
+    "local", "c1", "0s0", "0y0", "r0", "masked", "outmap", "1b0", "1s0", "0a1", "0s1", "0b1", "0y1", "0q01",
+    "0y2", "carry", "c2", "0s2", "0f0", "0q11", "r1", "1a0", "0q31", "0f1", "1y0", "0b2", "0y3", "0d0",
+    "0q02", "r2", "0f2", "0e0", "0y4", "0q21", "0d1", "far", "resp", "m", "0q12", "0q32", "0f3", "0e1",
+    "0d2", "1a1", "1f0", "0b3", "0y5", "0e2", "0f4", "0q03", "0y6", "0q22", "0d3", "0q13", "proj", "0q33",
+    "0f5", "0e3", "first0", "first1", "0b4", "0d4", "0y7", "first2", "first3", "0q04", "1b1", "1q01", "1s1",
+    "0f6", "0q23", "0e4", "first4", "0q34", "1y1", "0d5", "0q14", "1y2", "1s2", "1d0", "1b2", "1y3", "0e5",
+    "first5", "0f7", "1e0", "1q02", "0d6", "1q11", "1y4", "1q31", "0q24", "1f1", "0e6", "first6", "1q21",
+    "1f2", "1f3", "1b3", "1y5", "1q03", "1y6", "0d7", "1q12", "1f4", "1q32", "1d1", "1d2", "0e7", "first7",
+    "hidden", "1b4", "1q22", "1q04", "1d3", "1y7", "second0", "scat0", "1f5", "1e1", "second1", "scat1",
+    "1q13", "1e2", "second2", "scat2", "1q33", "1f6", "1e3", "second3", "scat3", "1d4", "1q23", "pass0",
+    "1f7", "pass1", "1d5", "1e4", "second4", "pass2", "scat4", "1q14", "1d6", "pass3", "1q34", "1e5",
+    "second5", "scat5", "1q24", "1d7", "fin0", "1e6", "second6", "scat6", "fin1", "fin2", "1e7", "second7",
+    "pass4", "scat7", "fin3", "pass5", "pass6", "fin4", "pass7", "fin5", "fin6", "fin7",
 )
 
 
@@ -77,10 +78,11 @@
 
 
 def kernel(
-    resid, mix, forget_t, decay, turn, in_re, in_im, out_re, out_im, skip, mix_gain, w_out, ffn_gain,
-    gate, up, down_t, out,
-    G, RA, WO, MX, X, RM, GA, UA, HB, PT, RS, UB, YB, ST, C1, C2,
-    send_sem, recv_sem, local_sem,
+    resid, mix_h, forget_h, decay_h, turn_h, in_re_h, in_im_h, out_re_h, out_im_h, skip_h, mix_gain_h,
+    w_out, ffn_gain_h, gate, up, down_t, out,
+    mix, forget_t, decay, turn, in_re, in_im, out_re, out_im, skip, mix_gain, ffn_gain,
+    G, RA, WO, MX, X, RM, GA, UA, HB, PT, RS, RB, UB, YB, ST, C1, C2,
+    send_sem, recv_sem, local_sem, entry_sem,
 ):
     me, x = lax.axis_index("sp"), lax.axis_index("tp")
     c = lax.rem(me, NC)
@@ -107,112 +109,128 @@
     zp, zm = at_sp(zr(1), y, c), at_sp(zr(-1), y, c)
     partner = at_sp(z, y, 1 - c)
 
-    numbers, pending = {}, []
-
-    def number(name):
-        return numbers.setdefault(name, len(numbers))
-
-    def send(name, src, dst, to):
-        k = number(name)
-        copy = pltpu.make_async_remote_copy(
-            src_ref=src, dst_ref=dst, send_sem=send_sem.at[k], recv_sem=recv_sem.at[k],
+    groups, arrivals = {}, {}
+
+    def send(group, name, src, dst, to):
+        k = groups.setdefault(group, len(groups))
+        n = arrivals.setdefault(name, len(arrivals))
+        pltpu.make_async_remote_copy(
+            src_ref=src, dst_ref=dst, send_sem=send_sem.at[k], recv_sem=recv_sem.at[n],
             device_id=to, device_id_type=MESH,
+        ).start()
+
+    def waiter(k, n, bytes_of):
+        return pltpu.make_async_remote_copy(
+            src_ref=bytes_of, dst_ref=bytes_of, send_sem=send_sem.at[k], recv_sem=recv_sem.at[n],
+            device_id=partner, device_id_type=MESH,
         )
-        copy.start()
-        pending.append(copy)
-
-    def recv(name, dst):
-        k = number(name)
-        pltpu.make_async_remote_copy(
-            src_ref=dst, dst_ref=dst, send_sem=send_sem.at[k], recv_sem=recv_sem.at[k],
-            device_id=partner, device_id_type=MESH,
-        ).wait_recv()
-
-    tasks = {}
+
+    def recv(name, bytes_of):
+        waiter(0, arrivals[name], bytes_of).wait_recv()
+
+    def sent(group, bytes_of):
+        waiter(groups[group], 0, bytes_of).wait_send()
+
+    tasks, drains = {}, []
 
     def task(f):
         tasks[f.__name__] = f
         return f
 
-    def block(p, dz, dy, lanes):
-        first, count = PHASES[p]
-        return G.at[
-            pl.ds(first, count), zr(dz), yr(dy), c, :, pl.ds(lanes[0], lanes[1] - lanes[0])
-        ]
-
     def gather_tasks(p):
         first, count = PHASES[p]
+        cut, cut_plus = PATH_A[p]
+        tiles = (HID - cut) // 128
+        few, many = cut + tiles // 2 * 128, cut + (tiles - tiles // 2) * 128
+        path_a, path_a1, path_a2 = (0, cut), (0, cut_plus), (cut_plus, cut)
+        path_b = (cut, HID)
+
+        def halves(odd):
+            middle = many if odd else few
+            return (cut, middle), (middle, HID)
+
+        def block(dz, dy, lanes):
+            return G.at[
+                pl.ds(first, count), zr(dz), yr(dy), c, :, pl.ds(lanes[0], lanes[1] - lanes[0])
+            ]
+
+        def sized(planes, rows, lanes):
+            return G.at[
+                pl.ds(first, count), pl.ds(0, planes), pl.ds(0, rows), c, :,
+                pl.ds(lanes[0], lanes[1] - lanes[0]),
+            ]
 
         def go(name, ref, to):
-            send(f"{p}{name}", ref, ref, to)
-
-        def got(name, ref):
-            recv(f"{p}{name}", ref)
+            send(f"{p}{name[0]}", f"{p}{name}", ref, ref, to)
 
         def both(name, ref, plus, minus):
-            go(name + "+", ref, plus)
-            go(name + "-", ref, minus)
+            go(name, ref, plus)
+            go(name, ref, minus)
+
+        def got(name, lanes, count_of=1):
+            recv(f"{p}{name}", sized(1, count_of, lanes))
 
         def a0():
-            both("A0", block(p, 0, 0, PATH_A), yp, ym)
+            both("A0", block(0, 0, path_a), yp, ym)
 
         def b0():
-            both("B1", block(p, 0, 0, PATH_B), zp, zm)
+            both("B1", block(0, 0, path_b), zp, zm)
 
         def a1():
-            got("A0+", block(p, 0, -1, PATH_A))
-            go("A1+", block(p, 0, -1, PATH_A1), yp)
-            got("A0-", block(p, 0, 1, PATH_A))
-            go("A1-", block(p, 0, 1, PATH_A2), ym)
+            got("A0", path_a, 2)
+            go("A1", block(0, -1, path_a1), yp)
+            go("A1", block(0, 1, path_a2), ym)
 
         def s0():
-            both("Z01", block(p, 0, 0, PATH_A), zp, zm)
+            both("Z01", block(0, 0, path_a), zp, zm)
 
         def s1():
-            both("Z11", block(p, 0, -1, PATH_A), zp, zm)
-            both("Z31", block(p, 0, 1, PATH_A), zp, zm)
+            both("Z11", block(0, -1, path_a), zp, zm)
+            both("Z31", block(0, 1, path_a), zp, zm)
 
         def s2():
-            got("A1+", block(p, 0, -2, PATH_A1))
-            got("A1-", block(p, 0, 2, PATH_A2))
-            both("Z21", block(p, 0, 2, PATH_A), zp, zm)
+            got("A1", path_a)
+            both("Z21", block(0, 2, path_a), zp, zm)
 
         def q(row, s):
             dy = (0, -1, 2, 1)[row]
-            if s < 4 or row in (0, 1):
-                got(f"Z{row}{s}+", block(p, -s, dy, PATH_A))
-                if s < 3 or (s == 3 and row in (0, 1)):
-                    go(f"Z{row}{s + 1}+", block(p, -s, dy, PATH_A), zp)
-            if s < 4 or row in (2, 3):
-                got(f"Z{row}{s}-", block(p, s, dy, PATH_A))
-                if s < 3 or (s == 3 and row in (2, 3)):
-                    go(f"Z{row}{s + 1}-", block(p, s, dy, PATH_A), zm)
+            got(f"Z{row}{s}", path_a, 2 if s < 4 else 1)
+            if s < 3 or (s == 3 and row in (0, 1)):
+                go(f"Z{row}{s + 1}", block(-s, dy, path_a), zp)
+            if s < 3 or (s == 3 and row in (2, 3)):
+                go(f"Z{row}{s + 1}", block(s, dy, path_a), zm)
 
         def b(s):
-            got(f"B{s}+", block(p, -s, 0, PATH_B if s < 4 else PATH_B1))
+            got(f"B{s}", path_b, 2 if s < 4 else 1)
+            plus, minus = (path_b, path_b) if s < 3 else halves(p)
             if s < 4:
-                go(f"B{s + 1}+", block(p, -s, 0, PATH_B if s < 3 else PATH_B1), zp)
-            got(f"B{s}-", block(p, s, 0, PATH_B if s < 4 else PATH_B2))
-            if s < 4:
-                go(f"B{s + 1}-", block(p, s, 0, PATH_B if s < 3 else PATH_B2), zm)
+                go(f"B{s + 1}", block(-s, 0, plus), zp)
+                go(f"B{s + 1}", block(s, 0, minus), zm)
 
         def y_(k):
-            both(f"Y{k}", block(p, PLANES[k], 0, PATH_B), yp, ym)
+            both(f"Y{k}", block(PLANES[k], 0, path_b), yp, ym)
 
         def f(k):
-            got(f"Y{k}+", block(p, PLANES[k], -1, PATH_B))
-            go(f"F{k}+", block(p, PLANES[k], -1, PATH_B1), yp)
-            got(f"Y{k}-", block(p, PLANES[k], 1, PATH_B))
-            go(f"F{k}-", block(p, PLANES[k], 1, PATH_B2), ym)
+            got(f"Y{k}", path_b, 2)
+            plus, minus = halves(k % 2)
+            go(f"F{k}", block(PLANES[k], -1, plus), yp)
+            go(f"F{k}", block(PLANES[k], 1, minus), ym)
 
         def d(k):
-            got(f"F{k}+", block(p, PLANES[k], -2, PATH_B1))
-            got(f"F{k}-", block(p, PLANES[k], 2, PATH_B2))
+            got(f"F{k}", path_b)
             go(f"D{k}", G.at[pl.ds(first, count), zr(PLANES[k]), :, c], partner)
 
         def e(k):
-            got(f"D{k}", G.at[pl.ds(first, count), zr(PLANES[k]), :, 1 - c])
-
+            recv(f"{p}D{k}", sized(1, NY, (0, HID)))
+
+        def all_sent():
+            for kind, planes, rows, lanes in (
+                ("A", 1, 3, path_a), ("Z", 7, 4, path_a), ("Y", 8, 2, path_b), ("F", 8, 1, path_b),
+                ("B", 7, 1, path_b), ("D", 8, 4, (0, HID)),
+            ):
+                sent(f"{p}{kind}", sized(planes, rows, lanes))
+
+        drains.append(all_sent)
         for name, f_ in (("a0", a0), ("b0", b0), ("a1", a1), ("s0", s0), ("s1", s1), ("s2", s2)):
             tasks[f"{p}{name}"] = f_
         for s in range(1, 5):
@@ -228,6 +246,16 @@
     for p in range(len(PHASES)):
         gather_tasks(p)
 
+    barrier = pltpu.get_barrier_semaphore()
+    peers = plane_peers + z_peers + x_peers
+    for peer in peers:
+        pl.semaphore_signal(barrier, inc=1, device_id=peer, device_id_type=MESH)
+    small = [
+        (mix_h, mix), (forget_h, forget_t), (decay_h, decay), (turn_h, turn), (in_re_h, in_re),
+        (in_im_h, in_im), (out_re_h, out_re), (out_im_h, out_im), (skip_h, skip),
+        (mix_gain_h, mix_gain), (ffn_gain_h, ffn_gain),
+    ]
+    early = [pltpu.make_async_copy(a, b, entry_sem.at[k]) for k, (a, b) in enumerate(small)]
     loads = [
         pltpu.make_async_copy(gate, G.at[0, z, y, c], local_sem.at[0]),
         pltpu.make_async_copy(up, G.at[1, z, y, c], local_sem.at[1]),
@@ -235,13 +263,18 @@
         pltpu.make_async_copy(resid, RA.at[x], local_sem.at[3]),
         pltpu.make_async_copy(w_out, WO, local_sem.at[4]),
     ]
-    for load in loads:
+    for load in loads[:3] + early + loads[3:]:
         load.start()
-    barrier = pltpu.get_barrier_semaphore()
-    peers = plane_peers + z_peers + x_peers
-    for peer in peers:
-        pl.semaphore_signal(barrier, inc=1, device_id=peer, device_id_type=MESH)
-
+
+    with jax.named_scope("entry"):
+        pl.semaphore_wait(barrier, len(peers))
+        for load in loads[:3]:
+            load.wait()
+    with jax.named_scope("opening"):
+        for name in OPENING:
+            tasks[name]()
+        for load in early:
+            load.wait()
     with jax.named_scope("prep"):
         drive = mix[...]
         spread = where_one(lax.rem(iota((CHAN, LOCAL), 1), CHAN) == iota((CHAN, LOCAL), 0))
@@ -278,10 +311,6 @@
         coarse = (iota((16, LANES), 0) - 8).astype(f32) * 16.0
         fine = iota((16, LANES), 0).astype(f32)
         centred = (iota((ROWS, LANES), 0) - ROWS // 2).astype(f32)
-    with jax.named_scope("entry"):
-        pl.semaphore_wait(barrier, len(peers))
-        for load in loads[:3]:
-            load.wait()
 
     def phase_tables(g):
         angle = turn2[g : g + 1]
@@ -324,7 +353,7 @@
     @task
     def c1():
         for d in range(1, NY * NC):
-            send(f"C1{d}", C1.at[slot], C1.at[slot], plane_peers[d - 1])
+            send("C1", "C1", C1.at[slot], C1.at[slot], plane_peers[d - 1])
 
     @task
     def masked():
@@ -337,8 +366,7 @@
     @task
     def carry():
         c_one, s_one = power(float(ROWS))
-        for d in range(1, NY * NC):
-            recv(f"C1{d}", C1.at[lax.rem(slot - d + NY * NC, NY * NC)])
+        recv("C1", C1.at[1:])
         acc = jnp.zeros((GROUPS, LANES), f32)
         log_acc = jnp.zeros((GROUPS, LANES), f32)
         before, log_before = acc, log_acc
@@ -356,7 +384,7 @@
     @task
     def c2():
         for d in range(1, NZ):
-            send(f"C2{d}", C2.at[z], C2.at[z], z_peers[d - 1])
+            send("C2", "C2", C2.at[z], C2.at[z], z_peers[d - 1])
 
     @task
     def outmap():
@@ -372,8 +400,7 @@
         c_plane, s_plane = power(float(ROWS * NY * NC))
         c_in, s_in = power(slot.astype(f32) * float(ROWS), v["log_before"])
         c_mid, s_mid = power(float(ROWS // 2 + 1))
-        for d in range(1, NZ):
-            recv(f"C2{d}", C2.at[zr(-d)])
+        recv("C2", C2.at[1:])
         total = jnp.zeros((GROUPS, LANES), f32)
         for j in range(NZ):
             step_on = jnp.exp(C2[j, GROUPS:]) * turned(total, c_plane, s_plane) + C2[j, 0:GROUPS]
@@ -392,33 +419,30 @@
     @task
     def m():
         for d in range(1, NX):
-            send(f"M{d}", MX.at[x], MX.at[x], x_peers[d - 1])
+            send("M", "M", MX.at[x], MX.at[x], x_peers[d - 1])
 
     half = OWN // 2
 
     @task
     def r0():
         loads[3].wait()
-        send("R+", RA.at[x], RA.at[x], x_peers[0])
-        send("R-", RA.at[x], RA.at[x], x_peers[2])
+        send("R", "R", RA.at[x], RA.at[x], x_peers[0])
+        send("R", "R", RA.at[x], RA.at[x], x_peers[2])
 
     @task
     def r1():
-        recv("R+", RA.at[xr(-1)])
-        send("Q+", RA.at[xr(-1), 0:half], RA.at[xr(-1), 0:half], x_peers[0])
-        recv("R-", RA.at[xr(1)])
-        send("Q-", RA.at[xr(1), half:], RA.at[xr(1), half:], x_peers[2])
+        recv("R", RA.at[2:])
+        send("Q", "Q", RA.at[xr(-1), 0:half], RA.at[xr(-1), 0:half], x_peers[0])
+        send("Q", "Q", RA.at[xr(1), half:], RA.at[xr(1), half:], x_peers[2])
 
     @task
     def r2():
-        recv("Q+", RA.at[xr(-2), 0:half])
-        recv("Q-", RA.at[xr(2), half:])
+        recv("Q", RA.at[0])
         loads[4].wait()
 
     @task
     def proj():
-        for d in range(1, NX):
-            recv(f"M{d}", MX.at[xr(-d)])
+        recv("M", MX.at[1:])
         mixed = [MX[q].astype(f32) for q in range(NX)]
         total = sum(jnp.sum(m * m, axis=1, keepdims=True) for m in mixed)
         scale = lax.rsqrt(total / float(LOCAL * NX) + eps)
@@ -458,17 +482,27 @@
         part = nt(HB[...], G[2, zr(PLANES[k])].reshape(ROWS, HID))
         PT[:, :, column_slice(k)] = part.astype(bf16).reshape(NX, OWN, ROWS)
 
+    def part_slice(k, side):
+        return pl.ds(pl.multiple_of(zr(PLANES[k]) * ROWS + 128 * side, 128), 128)
+
     def scat(k):
+        for side, to in ((0, x_peers[0]), (1, x_peers[2])):
+            send("S", f"S{k}", PT.at[xr(2), :, part_slice(k, side)], RB.at[k, side], to)
+
+    def pass_(k):
+        recv(f"S{k}", RB.at[k])
         cols = column_slice(k)
-        for d in range(1, NX):
-            send(f"S{k}{d}", PT.at[xr(d), :, cols], RS.at[x, :, cols], x_peers[d - 1])
+        for side, dx in ((0, 1), (1, -1)):
+            lanes = part_slice(k, side)
+            sum_ = PT[xr(dx), :, lanes].astype(f32) + RB[k, side].astype(f32)
+            PT[xr(dx), :, lanes] = sum_.astype(bf16)
+        send("V", f"V{k}", PT.at[xr(1), :, cols], RS.at[0, :, cols], x_peers[0])
+        send("V", f"V{k}", PT.at[xr(-1), :, cols], RS.at[1, :, cols], x_peers[2])
 
     def fin(k):
         cols = column_slice(k)
-        ffn = PT[x, :, cols].astype(f32)
-        for d in range(1, NX):
-            recv(f"S{k}{d}", RS.at[xr(-d), :, cols])
-            ffn = ffn + RS[xr(-d), :, cols].astype(f32)
+        recv(f"V{k}", RS.at[:, :, 0:ROWS])
+        ffn = PT[x, :, cols].astype(f32) + RS[0, :, cols].astype(f32) + RS[1, :, cols].astype(f32)
         kept = RM[pl.ds(pl.multiple_of(x * OWN, OWN), OWN), cols]
         out[:, cols] = (kept + 0.5 * ffn).astype(bf16)
 
@@ -476,29 +510,44 @@
         tasks[f"first{k}"] = functools.partial(first, k)
         tasks[f"second{k}"] = functools.partial(second, k)
         tasks[f"scat{k}"] = functools.partial(scat, k)
+        tasks[f"pass{k}"] = functools.partial(pass_, k)
         tasks[f"fin{k}"] = functools.partial(fin, k)
 
     for name in ORDER:
         with jax.named_scope(name):
             tasks[name]()
     with jax.named_scope("drain"):
-        for copy in pending:
-            copy.wait_send()
+        assert (len(groups), len(arrivals)) == (N_GROUPS, N_ARRIVALS)
+        for drain in drains:
+            drain()
+        sent("C1", C1.at[1:])
+        sent("C2", C2.at[1:])
+        sent("M", MX.at[1:])
+        sent("R", RA.at[2:])
+        sent("Q", RA.at[0])
+        sent("S", RB)
+        sent("V", RS)
 
 
 def per_device(
     resid, mix_in, decay_rate, turn_rate, forget, input_real, input_imag, output_real, output_imag,
     skip_gain, mix_gain, w_out, ffn_gain, gating_matrix, w_up, w_down,
 ):
-    vmem = pl.BlockSpec(memory_space=pltpu.VMEM)
-    anywhere = pl.BlockSpec(memory_space=pl.ANY)
-    n_sems = 256
+    operands = (
+        resid, mix_in, forget.T, decay_rate, turn_rate,
+        input_real.transpose(0, 2, 1).reshape(-1, STATE),
+        input_imag.transpose(0, 2, 1).reshape(-1, STATE),
+        output_real.reshape(-1, STATE), output_imag.reshape(-1, STATE),
+        skip_gain, mix_gain.reshape(1, -1), w_out, ffn_gain.reshape(1, -1),
+        gating_matrix, w_up, w_down.T,
+    )
+    own = [pltpu.VMEM(operands[k].shape, operands[k].dtype) for k in (*range(1, 11), 12)]
     return pl.pallas_call(
         kernel,
         out_shape=jax.ShapeDtypeStruct((OWN, D), bf16),
-        in_specs=[anywhere] + [vmem] * 10 + [anywhere, vmem] + [anywhere] * 3,
-        out_specs=vmem,
-        scratch_shapes=[
+        in_specs=[pl.BlockSpec(memory_space=pl.ANY)] * len(operands),
+        out_specs=pl.BlockSpec(memory_space=pltpu.VMEM),
+        scratch_shapes=own + [
             pltpu.VMEM((3, NZ, NY, NC, SHARD, HID), bf16),
             pltpu.VMEM((NX, OWN, D), bf16),
             pltpu.VMEM((LOCAL * NX, D), bf16),
@@ -509,27 +558,22 @@
             pltpu.VMEM((ROWS, HID), f32),
             pltpu.VMEM((ROWS, HID), bf16),
             pltpu.VMEM((NX, OWN, D), bf16),
-            pltpu.VMEM((NX, OWN, D), bf16),
+            pltpu.VMEM((2, OWN, D), bf16),
+            pltpu.VMEM((NZ, 2, OWN, 128), bf16),
             pltpu.VMEM((ROWS, WIDE), f32),
             pltpu.VMEM((ROWS, WIDE), f32),
             pltpu.VMEM((2, ROWS, WIDE), f32),
             pltpu.VMEM((NY * NC, 2 * GROUPS, LANES), f32),
             pltpu.VMEM((NZ, 2 * GROUPS, LANES), f32),
-            pltpu.SemaphoreType.DMA((n_sems,)),
-            pltpu.SemaphoreType.DMA((n_sems,)),
+            pltpu.SemaphoreType.DMA((N_GROUPS,)),
+            pltpu.SemaphoreType.DMA((N_ARRIVALS,)),
             pltpu.SemaphoreType.DMA((5,)),
+            pltpu.SemaphoreType.DMA((len(own),)),
         ],
         compiler_params=pltpu.CompilerParams(
             collective_id=0, has_side_effects=True, vmem_limit_bytes=60 * 1024 * 1024
         ),
-    )(
-        resid, mix_in, forget.T, decay_rate, turn_rate,
-        input_real.transpose(0, 2, 1).reshape(-1, STATE),
-        input_imag.transpose(0, 2, 1).reshape(-1, STATE),
-        output_real.reshape(-1, STATE), output_imag.reshape(-1, STATE),
-        skip_gain, mix_gain.reshape(1, -1), w_out, ffn_gain.reshape(1, -1),
-        gating_matrix, w_up, w_down.T,
-    )
+    )(*operands)
 
 
 def solution(mesh):

time: 79.8 us -> 75.6 us (0.947)
  Pallas kernels: 78 us -> 73.9 us
    pallas_call x1, Pallas kernels: 78 us -> 73.9 us  [per_device(): pl.pallas_call(kernel, out_shape=jax.ShapeDtypeStruct((OWN, D), bf16), in...]
where the time goes in v2:
time: 75.6 us; the launch traced here: 75.5 us
  Pallas kernels  73.9 us (98%)
  local copies, waits for them, and re-layouts  1.67 us (2%)
    pallas_call x1, Pallas kernels, per_device(): pl.pallas_call(kernel, out_shape=jax.ShapeDtypeStruct((OWN, D), bf16), in...  73.9 us
    unnamed x1, local copies, waits for them, and re-layouts  1.67 us

profile of v2, /device:TPU:1, one launch (start us, length us, event | category | flops | bytes accessed | tf_op | source)
XLA Modules:
  0.0 75.5 jit_solution(14998282997127065809)
XLA Ops:
  0.0 73.9 %shard_map.154 = bf16[64,2048]{1,0:T(8,128)(2,1)} custom-call(bf16[64,2048]{1,0:T(8,128)(2,1)} %resid.1, bf16[256,128]{1,0:T(8,128)(2,1)} %mix_h.1, f32[8,256]{1,0:T(8,128)} %bitcast.17, f32[8,64]{1,0:T(8,128)} %decay_h.1, f32[8,64]{1,0:T(8,128)} %turn_h.1, f32[128,64]{1,0:T(8,128)} %bitcast.13, f32[128,64]{1,0:T(8,128)} %bitcast.14, f32[128,64]{1,0:T(8,128)} %bitcast.15, ...), custom_call_target="tpu_custom_call" | custom-call | tf_op jit(solution)/shard_map/pallas_call | solution.py:545
  73.9 1.7 %copy.18 = bf16[64,2048]{1,0:T(8,128)(2,1)} copy(bf16[64,2048]{1,0:T(8,128)(2,1)} %shard_map.154) | data formatting | bytes 524288

commit v3 on v2

--- a/solution.py
+++ b/solution.py
@@ -22,22 +22,23 @@
 PATH_A = ((512, 256), (640, 384))
 PHASES = ((0, 2), (2, 1))
 PLANES = (0, -1, 1, -2, 2, -3, 3, 4)
-OPENING = ("0a0", "0b0",)
+OPENING = ("0a0", "1a0", "0b0", "1s0", "1y0",)
+DIRECT = ()
 N_GROUPS, N_ARRIVALS = 19, 113
 ORDER = (
-    "local", "c1", "0s0", "0y0", "r0", "masked", "outmap", "1b0", "1s0", "0a1", "0s1", "0b1", "0y1", "0q01",
-    "0y2", "carry", "c2", "0s2", "0f0", "0q11", "r1", "1a0", "0q31", "0f1", "1y0", "0b2", "0y3", "0d0",
-    "0q02", "r2", "0f2", "0e0", "0y4", "0q21", "0d1", "far", "resp", "m", "0q12", "0q32", "0f3", "0e1",
-    "0d2", "1a1", "1f0", "0b3", "0y5", "0e2", "0f4", "0q03", "0y6", "0q22", "0d3", "0q13", "proj", "0q33",
-    "0f5", "0e3", "first0", "first1", "0b4", "0d4", "0y7", "first2", "first3", "0q04", "1b1", "1q01", "1s1",
-    "0f6", "0q23", "0e4", "first4", "0q34", "1y1", "0d5", "0q14", "1y2", "1s2", "1d0", "1b2", "1y3", "0e5",
-    "first5", "0f7", "1e0", "1q02", "0d6", "1q11", "1y4", "1q31", "0q24", "1f1", "0e6", "first6", "1q21",
-    "1f2", "1f3", "1b3", "1y5", "1q03", "1y6", "0d7", "1q12", "1f4", "1q32", "1d1", "1d2", "0e7", "first7",
-    "hidden", "1b4", "1q22", "1q04", "1d3", "1y7", "second0", "scat0", "1f5", "1e1", "second1", "scat1",
-    "1q13", "1e2", "second2", "scat2", "1q33", "1f6", "1e3", "second3", "scat3", "1d4", "1q23", "pass0",
-    "1f7", "pass1", "1d5", "1e4", "second4", "pass2", "scat4", "1q14", "1d6", "pass3", "1q34", "1e5",
-    "second5", "scat5", "1q24", "1d7", "fin0", "1e6", "second6", "scat6", "fin1", "fin2", "1e7", "second7",
-    "pass4", "scat7", "fin3", "pass5", "pass6", "fin4", "pass7", "fin5", "fin6", "fin7",
+    "r0", "local", "c1", "1b0", "outmap", "0s0", "masked", "0y0", "0a1", "0s1", "0b1", "0y2", "0y1",
+    "carry", "c2", "r1", "0f0", "0s2", "0q11", "0q31", "0f2", "0b2", "0y4", "r2", "0y3", "0f1", "0d0",
+    "0q21", "far", "0e0", "0q12", "resp", "m", "0q01", "0d2", "0f4", "0q32", "1f0", "0b3", "0y5", "0y6",
+    "0e2", "0q22", "0f3", "0d1", "0q13", "0e1", "0q02", "0d4", "0q33", "proj", "0e4", "1a1", "0f5", "0b4",
+    "1q01", "first0", "first1", "first4", "0y7", "first2", "0q23", "1b1", "1y1", "0q14", "0d3", "1s2",
+    "1d0", "0q34", "0q03", "1y2", "0d5", "0e3", "first3", "1e0", "1s1", "0q24", "0f6", "0e5", "first5",
+    "0f7", "1b2", "1y3", "1f1", "1q21", "0q04", "1q11", "1f2", "1q31", "0d6", "1y4", "1b3", "1y5", "0d7",
+    "1q02", "1y6", "0e6", "first6", "1q12", "1f3", "1d1", "1q22", "1d2", "1q32", "0e7", "first7", "1b4",
+    "1y7", "hidden", "second0", "1e1", "1q03", "scat0", "second1", "scat1", "1f5", "1e2", "second2",
+    "scat2", "1q13", "1f4", "1q23", "1f6", "1d3", "1q33", "pass0", "1f7", "1q04", "pass1", "1d5", "1e3",
+    "second3", "scat3", "1d4", "1q14", "pass2", "1q24", "1d6", "1e5", "second5", "scat5", "1q34", "1d7",
+    "1e4", "second4", "fin0", "scat4", "1e6", "second6", "scat6", "fin1", "pass3", "1e7", "second7", "fin2",
+    "scat7", "pass5", "pass4", "pass6", "fin3", "pass7", "fin5", "fin4", "fin6", "fin7",
 )
 
 
@@ -81,8 +82,8 @@
     resid, mix_h, forget_h, decay_h, turn_h, in_re_h, in_im_h, out_re_h, out_im_h, skip_h, mix_gain_h,
     w_out, ffn_gain_h, gate, up, down_t, out,
     mix, forget_t, decay, turn, in_re, in_im, out_re, out_im, skip, mix_gain, ffn_gain,
-    G, RA, WO, MX, X, RM, GA, UA, HB, PT, RS, RB, UB, YB, ST, C1, C2,
-    send_sem, recv_sem, local_sem, entry_sem,
+    G, RA, WO, MX, X, RM, GA, UA, HB, PT, RS, RB, RT, OB, UB, YB, ST, C1, C2,
+    send_sem, recv_sem, local_sem, entry_sem, out_sem,
 ):
     me, x = lax.axis_index("sp"), lax.axis_index("tp")
     c = lax.rem(me, NC)
@@ -131,7 +132,7 @@
     def sent(group, bytes_of):
         waiter(groups[group], 0, bytes_of).wait_send()
 
-    tasks, drains = {}, []
+    tasks, drains, stores = {}, [], []
 
     def task(f):
         tasks[f.__name__] = f
@@ -325,6 +326,13 @@
         return size * jnp.cos(turn2 * n), size * jnp.sin(turn2 * n) * sign8
 
     v = {}
+    on_diagonal = iota((GROUPS, LANES), 0) == iota((GROUPS, LANES), 1)
+
+    def as_row(column):
+        return jnp.sum(jnp.where(on_diagonal, column, 0.0), axis=0, keepdims=True)
+
+    def as_column(row):
+        return jnp.sum(jnp.where(on_diagonal, row, 0.0), axis=1, keepdims=True)
 
     @task
     def local():
@@ -348,7 +356,7 @@
             jnp.where(iota((GROUPS, ROWS), 1) == ROWS - 1, run_log_t, 0.0), axis=1, keepdims=True
         )
         C1[slot, 0:GROUPS] = jnp.concatenate(ends, axis=0)
-        C1[slot, GROUPS:] = jnp.broadcast_to(last_col, (GROUPS, LANES))
+        C1[slot, GROUPS:] = as_row(last_col)
 
     @task
     def c1():
@@ -368,17 +376,17 @@
         c_one, s_one = power(float(ROWS))
         recv("C1", C1.at[1:])
         acc = jnp.zeros((GROUPS, LANES), f32)
-        log_acc = jnp.zeros((GROUPS, LANES), f32)
+        log_acc = jnp.zeros((GROUPS, 1), f32)
         before, log_before = acc, log_acc
         for j in range(NY * NC):
             here = slot == j
             before = jnp.where(here, acc, before)
             log_before = jnp.where(here, log_acc, log_before)
-            log_j = C1[j, GROUPS:]
+            log_j = as_column(C1[j, GROUPS:])
             acc = jnp.exp(log_j) * turned(acc, c_one, s_one) + C1[j, 0:GROUPS]
             log_acc = log_acc + log_j
         C2[z, 0:GROUPS] = acc
-        C2[z, GROUPS:] = log_acc
+        C2[z, GROUPS:] = as_row(log_acc)
         v["before"], v["log_before"] = before, log_before
 
     @task
@@ -403,7 +411,8 @@
         recv("C2", C2.at[1:])
         total = jnp.zeros((GROUPS, LANES), f32)
         for j in range(NZ):
-            step_on = jnp.exp(C2[j, GROUPS:]) * turned(total, c_plane, s_plane) + C2[j, 0:GROUPS]
+            fade = jnp.exp(as_column(C2[j, GROUPS:]))
+            step_on = fade * turned(total, c_plane, s_plane) + C2[j, 0:GROUPS]
             total = jnp.where(j < z, step_on, total)
         v["carry"] = turned(v["before"] + turned(total, c_in, s_in), c_mid, s_mid)
 
@@ -486,6 +495,11 @@
         return pl.ds(pl.multiple_of(zr(PLANES[k]) * ROWS + 128 * side, 128), 128)
 
     def scat(k):
+        if k in DIRECT:
+            cols = column_slice(k)
+            for d in (2, 1, 3):
+                send("T", f"S{k}", PT.at[xr(d), :, cols], RT.at[DIRECT.index(k), x], x_peers[d - 1])
+            return
         for side, to in ((0, x_peers[0]), (1, x_peers[2])):
             send("S", f"S{k}", PT.at[xr(2), :, part_slice(k, side)], RB.at[k, side], to)
 
@@ -501,10 +515,20 @@
 
     def fin(k):
         cols = column_slice(k)
-        recv(f"V{k}", RS.at[:, :, 0:ROWS])
-        ffn = PT[x, :, cols].astype(f32) + RS[0, :, cols].astype(f32) + RS[1, :, cols].astype(f32)
+        ffn = PT[x, :, cols].astype(f32)
+        if k in DIRECT:
+            n = DIRECT.index(k)
+            recv(f"S{k}", RT.at[n, 1:])
+            for d in range(1, NX):
+                ffn = ffn + RT[n, xr(d)].astype(f32)
+        else:
+            recv(f"V{k}", RS.at[:, :, 0:ROWS])
+            ffn = ffn + RS[0, :, cols].astype(f32) + RS[1, :, cols].astype(f32)
         kept = RM[pl.ds(pl.multiple_of(x * OWN, OWN), OWN), cols]
-        out[:, cols] = (kept + 0.5 * ffn).astype(bf16)
+        OB[:, cols] = (kept + 0.5 * ffn).astype(bf16)
+        copy = pltpu.make_async_copy(OB.at[:, cols], out.at[:, cols], out_sem.at[k])
+        copy.start()
+        stores.append(copy)
 
     for k in range(NZ):
         tasks[f"first{k}"] = functools.partial(first, k)
@@ -525,8 +549,13 @@
         sent("M", MX.at[1:])
         sent("R", RA.at[2:])
         sent("Q", RA.at[0])
-        sent("S", RB)
-        sent("V", RS)
+        stages = NZ - len(DIRECT)
+        sent("S", RB.at[0:stages])
+        sent("V", RS.at[:, :, 0 : stages * ROWS])
+        if DIRECT:
+            sent("T", RT.at[:, 1:])
+        for store in stores:
+            store.wait()
 
 
 def per_device(
@@ -546,7 +575,7 @@
         kernel,
         out_shape=jax.ShapeDtypeStruct((OWN, D), bf16),
         in_specs=[pl.BlockSpec(memory_space=pl.ANY)] * len(operands),
-        out_specs=pl.BlockSpec(memory_space=pltpu.VMEM),
+        out_specs=pl.BlockSpec(memory_space=pl.ANY),
         scratch_shapes=own + [
             pltpu.VMEM((3, NZ, NY, NC, SHARD, HID), bf16),
             pltpu.VMEM((NX, OWN, D), bf16),
@@ -560,15 +589,18 @@
             pltpu.VMEM((NX, OWN, D), bf16),
             pltpu.VMEM((2, OWN, D), bf16),
             pltpu.VMEM((NZ, 2, OWN, 128), bf16),
+            pltpu.VMEM((max(len(DIRECT), 1), NX, OWN, ROWS), bf16),
+            pltpu.VMEM((OWN, D), bf16),
             pltpu.VMEM((ROWS, WIDE), f32),
             pltpu.VMEM((ROWS, WIDE), f32),
             pltpu.VMEM((2, ROWS, WIDE), f32),
-            pltpu.VMEM((NY * NC, 2 * GROUPS, LANES), f32),
-            pltpu.VMEM((NZ, 2 * GROUPS, LANES), f32),
+            pltpu.VMEM((NY * NC, GROUPS + 1, LANES), f32),
+            pltpu.VMEM((NZ, GROUPS + 1, LANES), f32),
             pltpu.SemaphoreType.DMA((N_GROUPS,)),
             pltpu.SemaphoreType.DMA((N_ARRIVALS,)),
             pltpu.SemaphoreType.DMA((5,)),
             pltpu.SemaphoreType.DMA((len(own),)),
+            pltpu.SemaphoreType.DMA((NZ,)),
         ],
         compiler_params=pltpu.CompilerParams(
             collective_id=0, has_side_effects=True, vmem_limit_bytes=60 * 1024 * 1024

time: 75.6 us -> 73.7 us (0.975)
  Pallas kernels: 73.9 us -> 71.9 us
    pallas_call x1, Pallas kernels: 73.9 us -> 71.9 us  [per_device(): pl.pallas_call(kernel, out_shape=jax.ShapeDtypeStruct((OWN, D), bf16), in...]
where the time goes in v3:
time: 73.7 us; the launch traced here: 73.6 us
  Pallas kernels  71.9 us (98%)
  local copies, waits for them, and re-layouts  1.67 us (2%)
    pallas_call x1, Pallas kernels, per_device(): pl.pallas_call(kernel, out_shape=jax.ShapeDtypeStruct((OWN, D), bf16), in...  71.9 us
    unnamed x1, local copies, waits for them, and re-layouts  1.67 us

profile of v3, /device:TPU:1, one launch (start us, length us, event | category | flops | bytes accessed | tf_op | source)
XLA Modules:
  0.0 73.6 jit_solution(11083055996317499291)
XLA Ops:
  0.0 71.9 %shard_map.154 = bf16[64,2048]{1,0:T(8,128)(2,1)} custom-call(bf16[64,2048]{1,0:T(8,128)(2,1)} %resid.1, bf16[256,128]{1,0:T(8,128)(2,1)} %mix_h.1, f32[8,256]{1,0:T(8,128)} %bitcast.17, f32[8,64]{1,0:T(8,128)} %decay_h.1, f32[8,64]{1,0:T(8,128)} %turn_h.1, f32[128,64]{1,0:T(8,128)} %bitcast.13, f32[128,64]{1,0:T(8,128)} %bitcast.14, f32[128,64]{1,0:T(8,128)} %bitcast.15, ...), custom_call_target="tpu_custom_call" | custom-call | tf_op jit(solution)/shard_map/pallas_call | solution.py:574
  71.9 1.7 %copy.18 = bf16[64,2048]{1,0:T(8,128)(2,1)} copy(bf16[64,2048]{1,0:T(8,128)(2,1)} %shard_map.154) | data formatting | bytes 524288

commit v4 on v3

--- a/solution.py
+++ b/solution.py
@@ -22,23 +22,24 @@
 PATH_A = ((512, 256), (640, 384))
 PHASES = ((0, 2), (2, 1))
 PLANES = (0, -1, 1, -2, 2, -3, 3, 4)
-OPENING = ("0a0", "1a0", "0b0", "1s0", "1y0",)
+OPENING = ("1a0", "0a0", "0b0", "1y0",)
+RELAY = (7,)
 DIRECT = ()
-N_GROUPS, N_ARRIVALS = 19, 113
+N_GROUPS, N_ARRIVALS = 21, 114
 ORDER = (
-    "r0", "local", "c1", "1b0", "outmap", "0s0", "masked", "0y0", "0a1", "0s1", "0b1", "0y2", "0y1",
-    "carry", "c2", "r1", "0f0", "0s2", "0q11", "0q31", "0f2", "0b2", "0y4", "r2", "0y3", "0f1", "0d0",
-    "0q21", "far", "0e0", "0q12", "resp", "m", "0q01", "0d2", "0f4", "0q32", "1f0", "0b3", "0y5", "0y6",
-    "0e2", "0q22", "0f3", "0d1", "0q13", "0e1", "0q02", "0d4", "0q33", "proj", "0e4", "1a1", "0f5", "0b4",
-    "1q01", "first0", "first1", "first4", "0y7", "first2", "0q23", "1b1", "1y1", "0q14", "0d3", "1s2",
-    "1d0", "0q34", "0q03", "1y2", "0d5", "0e3", "first3", "1e0", "1s1", "0q24", "0f6", "0e5", "first5",
-    "0f7", "1b2", "1y3", "1f1", "1q21", "0q04", "1q11", "1f2", "1q31", "0d6", "1y4", "1b3", "1y5", "0d7",
-    "1q02", "1y6", "0e6", "first6", "1q12", "1f3", "1d1", "1q22", "1d2", "1q32", "0e7", "first7", "1b4",
-    "1y7", "hidden", "second0", "1e1", "1q03", "scat0", "second1", "scat1", "1f5", "1e2", "second2",
-    "scat2", "1q13", "1f4", "1q23", "1f6", "1d3", "1q33", "pass0", "1f7", "1q04", "pass1", "1d5", "1e3",
-    "second3", "scat3", "1d4", "1q14", "pass2", "1q24", "1d6", "1e5", "second5", "scat5", "1q34", "1d7",
-    "1e4", "second4", "fin0", "scat4", "1e6", "second6", "scat6", "fin1", "pass3", "1e7", "second7", "fin2",
-    "scat7", "pass5", "pass4", "pass6", "fin3", "pass7", "fin5", "fin4", "fin6", "fin7",
+    "r0", "local", "1b0", "c1", "masked", "outmap", "1s0", "0y0", "0s0", "0a1", "0s1", "0b1", "0y1", "1f0",
+    "h0", "carry", "r1", "h1", "0f0", "h2", "0s2", "c2", "0q11", "0y2", "0q31", "0f1", "0d0", "0b2", "0y4",
+    "0y3", "r2", "0e0", "0q21", "far", "resp", "m", "1q01", "0q32", "0f2", "0q01", "0d1", "0f4", "0b3",
+    "0y5", "0y6", "0e1", "0q22", "0d2", "0q12", "0e2", "0f3", "0q02", "0d4", "proj", "1a1", "1s1", "0b4",
+    "0y7", "first0", "first1", "0e4", "0q23", "first4", "first2", "0q13", "0f6", "0d3", "1b1", "1y1", "1s2",
+    "1d0", "0q03", "1y2", "1q11", "0e3", "first3", "1e0", "0f7", "0q33", "0q24", "0q14", "0d6", "0f5",
+    "1b2", "1y3", "1f1", "1q21", "1f2", "0e6", "first6", "0q04", "1q31", "1y4", "0q34", "0d7", "1q12",
+    "0d5", "1b3", "1y6", "1f3", "1q02", "1q22", "0e7", "first7", "1d1", "1y5", "1q32", "1d2", "0e5",
+    "first5", "hidden", "1b4", "1y7", "second0", "scat0", "1e1", "second1", "scat1", "1q03", "1d3", "1f6",
+    "1e2", "second2", "1q23", "scat2", "1q13", "1f4", "1f5", "1q33", "1e3", "second3", "1f7", "scat3",
+    "pass0", "1d6", "pass1", "1q04", "1d4", "pass2", "1q24", "1d5", "1q14", "1e6", "second6", "1q34", "1d7",
+    "scat6", "1e4", "second4", "scat4", "pass3", "1e5", "second5", "scat5", "fin0", "1e7", "second7",
+    "scat7", "fin1", "fin2", "pass6", "pass4", "fin3", "pass5", "pass7", "fin6", "fin4", "fin5", "fin7",
 )
 
 
@@ -82,8 +83,8 @@
     resid, mix_h, forget_h, decay_h, turn_h, in_re_h, in_im_h, out_re_h, out_im_h, skip_h, mix_gain_h,
     w_out, ffn_gain_h, gate, up, down_t, out,
     mix, forget_t, decay, turn, in_re, in_im, out_re, out_im, skip, mix_gain, ffn_gain,
-    G, RA, WO, MX, X, RM, GA, UA, HB, PT, RS, RB, RT, OB, UB, YB, ST, C1, C2,
-    send_sem, recv_sem, local_sem, entry_sem, out_sem,
+    G, RA, WO, MX, X, RM, GA, UA, HB, PT, RS, RB, RQ, RT, UB, YB, ST, C1, C2,
+    send_sem, recv_sem, local_sem, entry_sem, hello_sem,
 ):
     me, x = lax.axis_index("sp"), lax.axis_index("tp")
     c = lax.rem(me, NC)
@@ -132,7 +133,7 @@
     def sent(group, bytes_of):
         waiter(groups[group], 0, bytes_of).wait_send()
 
-    tasks, drains, stores = {}, [], []
+    tasks, drains = {}, []
 
     def task(f):
         tasks[f.__name__] = f
@@ -248,7 +249,7 @@
         gather_tasks(p)
 
     barrier = pltpu.get_barrier_semaphore()
-    peers = plane_peers + z_peers + x_peers
+    peers = plane_peers + [zp, zm] + x_peers
     for peer in peers:
         pl.semaphore_signal(barrier, inc=1, device_id=peer, device_id_type=MESH)
     small = [
@@ -259,18 +260,31 @@
     early = [pltpu.make_async_copy(a, b, entry_sem.at[k]) for k, (a, b) in enumerate(small)]
     loads = [
         pltpu.make_async_copy(gate, G.at[0, z, y, c], local_sem.at[0]),
-        pltpu.make_async_copy(up, G.at[1, z, y, c], local_sem.at[1]),
-        pltpu.make_async_copy(down_t, G.at[2, z, y, c], local_sem.at[2]),
-        pltpu.make_async_copy(resid, RA.at[x], local_sem.at[3]),
-        pltpu.make_async_copy(w_out, WO, local_sem.at[4]),
+        pltpu.make_async_copy(up, G.at[1, z, y, c], local_sem.at[0]),
+        pltpu.make_async_copy(down_t, G.at[2, z, y, c], local_sem.at[0]),
+        pltpu.make_async_copy(resid, RA.at[x], local_sem.at[1]),
+        pltpu.make_async_copy(w_out, WO, local_sem.at[2]),
     ]
     for load in loads[:3] + early + loads[3:]:
         load.start()
 
+    def hello(n):
+        for peer in (zp, zm):
+            pl.semaphore_signal(hello_sem.at[n], inc=1, device_id=peer, device_id_type=MESH)
+
+    def met(n):
+        pl.semaphore_wait(hello_sem.at[n], 2)
+        if n < 2:
+            hello(n + 1)
+
+    for n in range(3):
+        tasks[f"h{n}"] = functools.partial(met, n)
+
     with jax.named_scope("entry"):
         pl.semaphore_wait(barrier, len(peers))
-        for load in loads[:3]:
-            load.wait()
+        own_weights = G.at[:, z, y, c]
+        pltpu.make_async_copy(own_weights, own_weights, local_sem.at[0]).wait()
+        hello(0)
     with jax.named_scope("opening"):
         for name in OPENING:
             tasks[name]()
@@ -502,16 +516,26 @@
             return
         for side, to in ((0, x_peers[0]), (1, x_peers[2])):
             send("S", f"S{k}", PT.at[xr(2), :, part_slice(k, side)], RB.at[k, side], to)
+        if k in RELAY:
+            near(k, "W")
+
+    def near(k, kind):
+        cols = column_slice(k)
+        send(kind, f"{kind}{k}", PT.at[xr(1), :, cols], RS.at[0, :, cols], x_peers[0])
+        send(kind, f"{kind}{k}", PT.at[xr(-1), :, cols], RS.at[1, :, cols], x_peers[2])
 
     def pass_(k):
         recv(f"S{k}", RB.at[k])
-        cols = column_slice(k)
+        if k in RELAY:
+            n = RELAY.index(k)
+            for side, to in ((0, x_peers[0]), (1, x_peers[2])):
+                send("U", f"V{k}", RB.at[k, side], RQ.at[n, side], to)
+            return
         for side, dx in ((0, 1), (1, -1)):
             lanes = part_slice(k, side)
             sum_ = PT[xr(dx), :, lanes].astype(f32) + RB[k, side].astype(f32)
             PT[xr(dx), :, lanes] = sum_.astype(bf16)
-        send("V", f"V{k}", PT.at[xr(1), :, cols], RS.at[0, :, cols], x_peers[0])
-        send("V", f"V{k}", PT.at[xr(-1), :, cols], RS.at[1, :, cols], x_peers[2])
+        near(k, "V")
 
     def fin(k):
         cols = column_slice(k)
@@ -522,13 +546,14 @@
             for d in range(1, NX):
                 ffn = ffn + RT[n, xr(d)].astype(f32)
         else:
-            recv(f"V{k}", RS.at[:, :, 0:ROWS])
+            recv(f"W{k}" if k in RELAY else f"V{k}", RS.at[:, :, 0:ROWS])
             ffn = ffn + RS[0, :, cols].astype(f32) + RS[1, :, cols].astype(f32)
+        if k in RELAY:
+            n = RELAY.index(k)
+            recv(f"V{k}", RQ.at[n])
+            ffn = ffn + jnp.concatenate([RQ[n, 0], RQ[n, 1]], axis=1).astype(f32)
         kept = RM[pl.ds(pl.multiple_of(x * OWN, OWN), OWN), cols]
-        OB[:, cols] = (kept + 0.5 * ffn).astype(bf16)
-        copy = pltpu.make_async_copy(OB.at[:, cols], out.at[:, cols], out_sem.at[k])
-        copy.start()
-        stores.append(copy)
+        out[:, cols] = (kept + 0.5 * ffn).astype(bf16)
 
     for k in range(NZ):
         tasks[f"first{k}"] = functools.partial(first, k)
@@ -549,13 +574,15 @@
         sent("M", MX.at[1:])
         sent("R", RA.at[2:])
         sent("Q", RA.at[0])
-        stages = NZ - len(DIRECT)
-        sent("S", RB.at[0:stages])
-        sent("V", RS.at[:, :, 0 : stages * ROWS])
+        passed = NZ - len(DIRECT)
+        summed = passed - len(RELAY)
+        sent("S", RB.at[0:passed])
+        sent("V", RS.at[:, :, 0 : summed * ROWS])
         if DIRECT:
             sent("T", RT.at[:, 1:])
-        for store in stores:
-            store.wait()
+        if RELAY:
+            sent("W", RS.at[:, :, 0 : len(RELAY) * ROWS])
+            sent("U", RQ)
 
 
 def per_device(
@@ -575,7 +602,7 @@
         kernel,
         out_shape=jax.ShapeDtypeStruct((OWN, D), bf16),
         in_specs=[pl.BlockSpec(memory_space=pl.ANY)] * len(operands),
-        out_specs=pl.BlockSpec(memory_space=pl.ANY),
+        out_specs=pl.BlockSpec(memory_space=pltpu.VMEM),
         scratch_shapes=own + [
             pltpu.VMEM((3, NZ, NY, NC, SHARD, HID), bf16),
             pltpu.VMEM((NX, OWN, D), bf16),
@@ -589,8 +616,8 @@
             pltpu.VMEM((NX, OWN, D), bf16),
             pltpu.VMEM((2, OWN, D), bf16),
             pltpu.VMEM((NZ, 2, OWN, 128), bf16),
+            pltpu.VMEM((max(len(RELAY), 1), 2, OWN, 128), bf16),
             pltpu.VMEM((max(len(DIRECT), 1), NX, OWN, ROWS), bf16),
-            pltpu.VMEM((OWN, D), bf16),
             pltpu.VMEM((ROWS, WIDE), f32),
             pltpu.VMEM((ROWS, WIDE), f32),
             pltpu.VMEM((2, ROWS, WIDE), f32),
@@ -598,14 +625,14 @@
             pltpu.VMEM((NZ, GROUPS + 1, LANES), f32),
             pltpu.SemaphoreType.DMA((N_GROUPS,)),
             pltpu.SemaphoreType.DMA((N_ARRIVALS,)),
-            pltpu.SemaphoreType.DMA((5,)),
+            pltpu.SemaphoreType.DMA((3,)),
             pltpu.SemaphoreType.DMA((len(own),)),
-            pltpu.SemaphoreType.DMA((NZ,)),
+            pltpu.SemaphoreType.REGULAR((3,)),
         ],
         compiler_params=pltpu.CompilerParams(
-            collective_id=0, has_side_effects=True, vmem_limit_bytes=60 * 1024 * 1024
+            collective_id=0, has_side_effects=True, vmem_limit_bytes=52 * 1024 * 1024
         ),
-    )(*operands)
+    )(*[pltpu.with_memory_space_constraint(operand, pltpu.HBM) for operand in operands])
 
 
 def solution(mesh):

time: 73.7 us -> 71.4 us (0.969)
  Pallas kernels: 71.9 us -> 70.6 us
  local copies, waits for them, and re-layouts: 1.67 us -> 0.71 us
    pallas_call x1, Pallas kernels: 71.9 us -> 70.6 us  [per_device(): pl.pallas_call(kernel, out_shape=jax.ShapeDtypeStruct((OWN, D), bf16), in...]
    unnamed x1, local copies, waits for them, and re-layouts: 1.67 us -> 0.71 us
where the time goes in v4:
time: 71.4 us; the launch traced here: 71.3 us
  Pallas kernels  70.6 us (99%)
    pallas_call x1, Pallas kernels, per_device(): pl.pallas_call(kernel, out_shape=jax.ShapeDtypeStruct((OWN, D), bf16), in...  70.6 us

profile of v4, /device:TPU:1, one launch (start us, length us, event | category | flops | bytes accessed | tf_op | source)
XLA Modules:
  0.0 71.3 jit_solution(15170337835726269833)
XLA Ops:
  0.0 70.6 %shard_map.154 = bf16[64,2048]{1,0:T(8,128)(2,1)S(1)} custom-call(bf16[64,2048]{1,0:T(8,128)(2,1)} %resid.1, bf16[256,128]{1,0:T(8,128)(2,1)} %mix_h.1, f32[8,256]{1,0:T(8,128)} %bitcast.17, f32[8,64]{1,0:T(8,128)} %decay_h.1, f32[8,64]{1,0:T(8,128)} %turn_h.1, f32[128,64]{1,0:T(8,128)} %bitcast.13, f32[128,64]{1,0:T(8,128)} %bitcast.14, ...), custom_call_target="tpu_custom_call" | custom-call | tf_op jit(solution)/shard_map/pallas_call | solution.py:601
  70.6 0.7 copy.18

commit v5 on v4

--- a/solution.py
+++ b/solution.py
@@ -25,7 +25,7 @@
 OPENING = ("1a0", "0a0", "0b0", "1y0",)
 RELAY = (7,)
 DIRECT = ()
-N_GROUPS, N_ARRIVALS = 21, 114
+N_GROUPS = 21
 ORDER = (
     "r0", "local", "1b0", "c1", "masked", "outmap", "1s0", "0y0", "0s0", "0a1", "0s1", "0b1", "0y1", "1f0",
     "h0", "carry", "r1", "h1", "0f0", "h2", "0s2", "c2", "0q11", "0y2", "0q31", "0f1", "0d0", "0b2", "0y4",
@@ -41,6 +41,56 @@
     "scat6", "1e4", "second4", "scat4", "pass3", "1e5", "second5", "scat5", "fin0", "1e7", "second7",
     "scat7", "fin1", "fin2", "pass6", "pass4", "fin3", "pass5", "pass7", "fin6", "fin4", "fin5", "fin7",
 )
+ARRIVALS = (
+    ("1A0", "1Y2", "1Y7"),
+    ("0A0", "0Y2", "0F3", "1F1", "1F5"),
+    ("0B1", "0B3", "1B2", "1B4"),
+    ("1Y0", "0Y3", "1Y1", "1Y5"),
+    ("R", "S0", "S7"),
+    ("1B1", "1B3", "1Z14"),
+    ("C1",),
+    ("1Z01", "1Z31", "1Z33"),
+    ("0Y0", "0Y4", "1A1", "1Y4"),
+    ("0Z01", "0Z03"),
+    ("0A1", "0F2", "1Y3", "1F6"),
+    ("0Z11", "0Z02", "0Z04"),
+    ("0Z31", "0Z33"),
+    ("0B2", "0B4"),
+    ("0Y1", "0Y5", "1Y6"),
+    ("1F0", "1F2", "1F7"),
+    ("Q", "V0", "V7"),
+    ("0F0", "0F4", "0F7"),
+    ("0Z21", "0Z23", "1Z32", "1Z34"),
+    ("C2",),
+    ("0Z12", "0Z14", "1Z03"),
+    ("0Z32", "1Z11", "1Z13"),
+    ("0F1", "0Y7"),
+    ("0D0", "0D2", "0D3", "0D5", "1D4"),
+    ("0Z22", "0Z24"),
+    ("M",),
+    ("1Z02", "1Z04"),
+    ("0D1", "0D4", "0D6", "1D1", "1D6"),
+    ("0Y6", "0F5", "1F4"),
+    ("0Z13", "1Z22", "1Z24"),
+    ("0F6", "1F3"),
+    ("1Z21", "1Z23"),
+    ("1D0", "0D7", "1D3", "1D7"),
+    ("1Z12",),
+    ("0Z34",),
+    ("1D2",),
+    ("S1", "V4"),
+    ("S2", "V6"),
+    ("S3", "V5"),
+    ("V1",),
+    ("V2",),
+    ("1D5",),
+    ("S6",),
+    ("S4",),
+    ("V3",),
+    ("S5",),
+    ("W7",),
+)
+ARRIVAL_OF = {name: k for k, names in enumerate(ARRIVALS) for name in names}
 
 
 def iota(shape, dim):
@@ -111,11 +161,11 @@
     zp, zm = at_sp(zr(1), y, c), at_sp(zr(-1), y, c)
     partner = at_sp(z, y, 1 - c)
 
-    groups, arrivals = {}, {}
+    groups = {}
 
     def send(group, name, src, dst, to):
         k = groups.setdefault(group, len(groups))
-        n = arrivals.setdefault(name, len(arrivals))
+        n = ARRIVAL_OF[name]
         pltpu.make_async_remote_copy(
             src_ref=src, dst_ref=dst, send_sem=send_sem.at[k], recv_sem=recv_sem.at[n],
             device_id=to, device_id_type=MESH,
@@ -128,7 +178,7 @@
         )
 
     def recv(name, bytes_of):
-        waiter(0, arrivals[name], bytes_of).wait_recv()
+        waiter(0, ARRIVAL_OF[name], bytes_of).wait_recv()
 
     def sent(group, bytes_of):
         waiter(groups[group], 0, bytes_of).wait_send()
@@ -566,7 +616,7 @@
         with jax.named_scope(name):
             tasks[name]()
     with jax.named_scope("drain"):
-        assert (len(groups), len(arrivals)) == (N_GROUPS, N_ARRIVALS)
+        assert len(groups) == N_GROUPS
         for drain in drains:
             drain()
         sent("C1", C1.at[1:])
@@ -624,7 +674,7 @@
             pltpu.VMEM((NY * NC, GROUPS + 1, LANES), f32),
             pltpu.VMEM((NZ, GROUPS + 1, LANES), f32),
             pltpu.SemaphoreType.DMA((N_GROUPS,)),
-            pltpu.SemaphoreType.DMA((N_ARRIVALS,)),
+            pltpu.SemaphoreType.DMA((len(ARRIVALS),)),
             pltpu.SemaphoreType.DMA((3,)),
             pltpu.SemaphoreType.DMA((len(own),)),
             pltpu.SemaphoreType.REGULAR((3,)),

time: 71.4 us -> 70.8 us (level)
  no operation moved by 1% of the time
where the time goes in v5:
time: 70.8 us; the launch traced here: 70.7 us
  Pallas kernels  70 us (99%)
  local copies, waits for them, and re-layouts  0.71 us (1%)
    pallas_call x1, Pallas kernels, per_device(): pl.pallas_call(kernel, out_shape=jax.ShapeDtypeStruct((OWN, D), bf16), in...  70 us

profile of v5, /device:TPU:1, one launch (start us, length us, event | category | flops | bytes accessed | tf_op | source)
XLA Modules:
  0.0 70.7 jit_solution(5851352842459989695)
XLA Ops:
  0.0 70.0 %shard_map.154 = bf16[64,2048]{1,0:T(8,128)(2,1)S(1)} custom-call(bf16[64,2048]{1,0:T(8,128)(2,1)} %resid.1, bf16[256,128]{1,0:T(8,128)(2,1)} %mix_h.1, f32[8,256]{1,0:T(8,128)} %bitcast.17, f32[8,64]{1,0:T(8,128)} %decay_h.1, f32[8,64]{1,0:T(8,128)} %turn_h.1, f32[128,64]{1,0:T(8,128)} %bitcast.13, f32[128,64]{1,0:T(8,128)} %bitcast.14, ...), custom_call_target="tpu_custom_call" | custom-call | tf_op jit(solution)/shard_map/pallas_call | solution.py:651
  70.0 0.7 copy.18

commit v6 on v4

--- a/solution.py
+++ b/solution.py
@@ -22,24 +22,26 @@
 PATH_A = ((512, 256), (640, 384))
 PHASES = ((0, 2), (2, 1))
 PLANES = (0, -1, 1, -2, 2, -3, 3, 4)
-OPENING = ("1a0", "0a0", "0b0", "1y0",)
+OPENING = (58, 0, 1, 84, 3)
 RELAY = (7,)
 DIRECT = ()
-N_GROUPS, N_ARRIVALS = 21, 114
+N_GROUPS, N_ARRIVALS = 21, 47
 ORDER = (
-    "r0", "local", "1b0", "c1", "masked", "outmap", "1s0", "0y0", "0s0", "0a1", "0s1", "0b1", "0y1", "1f0",
-    "h0", "carry", "r1", "h1", "0f0", "h2", "0s2", "c2", "0q11", "0y2", "0q31", "0f1", "0d0", "0b2", "0y4",
-    "0y3", "r2", "0e0", "0q21", "far", "resp", "m", "1q01", "0q32", "0f2", "0q01", "0d1", "0f4", "0b3",
-    "0y5", "0y6", "0e1", "0q22", "0d2", "0q12", "0e2", "0f3", "0q02", "0d4", "proj", "1a1", "1s1", "0b4",
-    "0y7", "first0", "first1", "0e4", "0q23", "first4", "first2", "0q13", "0f6", "0d3", "1b1", "1y1", "1s2",
-    "1d0", "0q03", "1y2", "1q11", "0e3", "first3", "1e0", "0f7", "0q33", "0q24", "0q14", "0d6", "0f5",
-    "1b2", "1y3", "1f1", "1q21", "1f2", "0e6", "first6", "0q04", "1q31", "1y4", "0q34", "0d7", "1q12",
-    "0d5", "1b3", "1y6", "1f3", "1q02", "1q22", "0e7", "first7", "1d1", "1y5", "1q32", "1d2", "0e5",
-    "first5", "hidden", "1b4", "1y7", "second0", "scat0", "1e1", "second1", "scat1", "1q03", "1d3", "1f6",
-    "1e2", "second2", "1q23", "scat2", "1q13", "1f4", "1f5", "1q33", "1e3", "second3", "1f7", "scat3",
-    "pass0", "1d6", "pass1", "1q04", "1d4", "pass2", "1q24", "1d5", "1q14", "1e6", "second6", "1q34", "1d7",
-    "scat6", "1e4", "second4", "scat4", "pass3", "1e5", "second5", "scat5", "fin0", "1e7", "second7",
-    "scat7", "fin1", "fin2", "pass6", "pass4", "fin3", "pass5", "pass7", "fin6", "fin4", "fin5", "fin7",
+    128, 119, 120, 124, 121, 61, 26, 59, 2, 4, 6, 30, 85, 116, 122, 129, 117, 27, 118, 5, 123, 34,
+    8, 10, 31, 28, 11, 42, 38, 130, 29, 9, 35, 125, 126, 127, 65, 15, 43, 7, 32, 16, 46, 50, 14, 33,
+    36, 39, 13, 37, 12, 44, 131, 60, 62, 21, 54, 133, 138, 45, 153, 19, 51, 143, 18, 40, 64, 88, 63,
+    86, 17, 92, 66, 41, 148, 87, 55, 24, 20, 23, 52, 47, 69, 96, 89, 67, 93, 53, 163, 22, 100, 68,
+    25, 56, 71, 48, 74, 108, 97, 70, 72, 57, 168, 90, 73, 94, 104, 49, 158, 132, 79, 112, 134, 135,
+    91, 139, 109, 98, 140, 75, 95, 144, 77, 76, 145, 101, 105, 78, 99, 149, 113, 150, 136, 110, 141,
+    80, 102, 146, 82, 106, 81, 111, 164, 83, 114, 165, 103, 154, 155, 151, 107, 159, 160, 137, 115,
+    169, 170, 142, 147, 166, 156, 152, 161, 171, 167, 157, 162, 172,
+)
+ARRIVALS = (
+    0, 1, 2, 3, 4, 5, 6, 7, 8, 9, 10, 11, 12, 13, 14, 15, 16, 17, 18, 19, 1, 20, 21, 22, 23, 2, 8,
+    3, 24, 10, 25, 26, 12, 17, 11, 27, 13, 14, 28, 18, 23, 1, 29, 4, 27, 8, 21, 7, 30, 24, 22, 20,
+    23, 2, 3, 31, 32, 11, 0, 33, 17, 34, 27, 28, 9, 10, 1, 29, 15, 8, 18, 32, 21, 23, 2, 14, 22, 20,
+    31, 27, 7, 35, 0, 3, 5, 28, 32, 36, 26, 29, 9, 37, 10, 15, 18, 1, 38, 16, 27, 39, 23, 40, 41,
+    32, 42, 43, 44, 45, 5, 46, 37, 36, 38, 16,
 )
 
 
@@ -115,7 +117,7 @@
 
     def send(group, name, src, dst, to):
         k = groups.setdefault(group, len(groups))
-        n = arrivals.setdefault(name, len(arrivals))
+        n = ARRIVALS[arrivals.setdefault(name, len(arrivals))]
         pltpu.make_async_remote_copy(
             src_ref=src, dst_ref=dst, send_sem=send_sem.at[k], recv_sem=recv_sem.at[n],
             device_id=to, device_id_type=MESH,
@@ -128,7 +130,7 @@
         )
 
     def recv(name, bytes_of):
-        waiter(0, arrivals[name], bytes_of).wait_recv()
+        waiter(0, ARRIVALS[arrivals[name]], bytes_of).wait_recv()
 
     def sent(group, bytes_of):
         waiter(groups[group], 0, bytes_of).wait_send()
@@ -286,8 +288,8 @@
         pltpu.make_async_copy(own_weights, own_weights, local_sem.at[0]).wait()
         hello(0)
     with jax.named_scope("opening"):
-        for name in OPENING:
-            tasks[name]()
+        for task_number in OPENING:
+            list(tasks.values())[task_number]()
         for load in early:
             load.wait()
     with jax.named_scope("prep"):
@@ -562,11 +564,12 @@
         tasks[f"pass{k}"] = functools.partial(pass_, k)
         tasks[f"fin{k}"] = functools.partial(fin, k)
 
-    for name in ORDER:
-        with jax.named_scope(name):
-            tasks[name]()
+    table = list(tasks)
+    for task_number in ORDER:
+        with jax.named_scope(table[task_number]):
+            tasks[table[task_number]]()
     with jax.named_scope("drain"):
-        assert (len(groups), len(arrivals)) == (N_GROUPS, N_ARRIVALS)
+        assert len(groups) == N_GROUPS and len(arrivals) == len(ARRIVALS)
         for drain in drains:
             drain()
         sent("C1", C1.at[1:])

time: 71.4 us -> 70.5 us (0.987)
  Pallas kernels: 70.6 us -> 69.7 us
    pallas_call x1, Pallas kernels: 70.6 us -> 69.7 us  [per_device(): pl.pallas_call(kernel, out_shape=jax.ShapeDtypeStruct((OWN, D), bf16), in...]
where the time goes in v6:
time: 70.5 us; the launch traced here: 70.4 us
  Pallas kernels  69.7 us (99%)
  local copies, waits for them, and re-layouts  0.71 us (1%)
    pallas_call x1, Pallas kernels, per_device(): pl.pallas_call(kernel, out_shape=jax.ShapeDtypeStruct((OWN, D), bf16), in...  69.7 us

profile of v6, /device:TPU:1, one launch (start us, length us, event | category | flops | bytes accessed | tf_op | source)
XLA Modules:
  0.0 70.4 jit_solution(10364597855024889126)
XLA Ops:
  0.0 69.7 %shard_map.154 = bf16[64,2048]{1,0:T(8,128)(2,1)S(1)} custom-call(bf16[64,2048]{1,0:T(8,128)(2,1)} %resid.1, bf16[256,128]{1,0:T(8,128)(2,1)} %mix_h.1, f32[8,256]{1,0:T(8,128)} %bitcast.17, f32[8,64]{1,0:T(8,128)} %decay_h.1, f32[8,64]{1,0:T(8,128)} %turn_h.1, f32[128,64]{1,0:T(8,128)} %bitcast.13, f32[128,64]{1,0:T(8,128)} %bitcast.14, ...), custom_call_target="tpu_custom_call" | custom-call | tf_op jit(solution)/shard_map/pallas_call | solution.py:604
  69.7 0.7 %copy.18 = bf16[64,2048]{1,0:T(8,128)(2,1)} copy(bf16[64,2048]{1,0:T(8,128)(2,1)S(1)} %shard_map.154) | data formatting | bytes 524288

commit v7 on v6

--- a/solution.py
+++ b/solution.py
@@ -250,10 +250,6 @@
     for p in range(len(PHASES)):
         gather_tasks(p)
 
-    barrier = pltpu.get_barrier_semaphore()
-    peers = plane_peers + [zp, zm] + x_peers
-    for peer in peers:
-        pl.semaphore_signal(barrier, inc=1, device_id=peer, device_id_type=MESH)
     small = [
         (mix_h, mix), (forget_h, forget_t), (decay_h, decay), (turn_h, turn), (in_re_h, in_re),
         (in_im_h, in_im), (out_re_h, out_re), (out_im_h, out_im), (skip_h, skip),
@@ -267,7 +263,13 @@
         pltpu.make_async_copy(resid, RA.at[x], local_sem.at[1]),
         pltpu.make_async_copy(w_out, WO, local_sem.at[2]),
     ]
-    for load in loads[:3] + early + loads[3:]:
+    for load in loads[:3]:
+        load.start()
+    barrier = pltpu.get_barrier_semaphore()
+    peers = plane_peers + [zp, zm] + x_peers
+    for peer in peers:
+        pl.semaphore_signal(barrier, inc=1, device_id=peer, device_id_type=MESH)
+    for load in early + loads[3:]:
         load.start()
 
     def hello(n):

time: 70.5 us -> 70.4 us (level)
  no operation moved by 1% of the time
where the time goes in v7:
time: 70.4 us
  Pallas kernels  69.7 us (99%)
  local copies, waits for them, and re-layouts  0.71 us (1%)
    pallas_call x1, Pallas kernels, per_device(): pl.pallas_call(kernel, out_shape=jax.ShapeDtypeStruct((OWN, D), bf16), in...  69.7 us

profile of v7, /device:TPU:1, one launch (start us, length us, event | category | flops | bytes accessed | tf_op | source)
XLA Modules:
  0.0 70.4 jit_solution(1271681783177385195)
XLA Ops:
  0.0 69.7 %shard_map.154 = bf16[64,2048]{1,0:T(8,128)(2,1)S(1)} custom-call(bf16[64,2048]{1,0:T(8,128)(2,1)} %resid.1, bf16[256,128]{1,0:T(8,128)(2,1)} %mix_h.1, f32[8,256]{1,0:T(8,128)} %bitcast.17, f32[8,64]{1,0:T(8,128)} %decay_h.1, f32[8,64]{1,0:T(8,128)} %turn_h.1, f32[128,64]{1,0:T(8,128)} %bitcast.13, f32[128,64]{1,0:T(8,128)} %bitcast.14, ...), custom_call_target="tpu_custom_call" | custom-call | tf_op jit(solution)/shard_map/pallas_call | solution.py:606
  69.7 0.7 %copy.18 = bf16[64,2048]{1,0:T(8,128)(2,1)} copy(bf16[64,2048]{1,0:T(8,128)(2,1)S(1)} %shard_map.154) | data formatting | bytes 524288
